TPU v7x, 32 devices: a whole 2x2x4 slice. The times are simulated.
32 devices in a mesh: rep: 2 (over x), fs: 8 (over z, y), tp: 2 (over core).
Axes of the slice: x: 2, y: 2, z: 4, core: 2. Of those that a mesh axis runs over, the one named last changes fastest.
Arguments:
- inputs: bfloat16 [4096, 2048], P(('rep', 'fs', 'tp')), may hold values from -6 to 6
- cotangent: bfloat16 [4096, 2048], P(('rep', 'fs', 'tp')), may hold values from -6 to 6
- up_weight: bfloat16 [2048, 4096], P('fs', 'tp'), may hold values from -0.125 to 0.125
- down_weight: bfloat16 [4096, 2048], P('tp', 'fs'), may hold values from -0.09375 to 0.09375
Outputs:
- input_grad: bfloat16 [4096, 2048], P(('rep', 'fs', 'tp'))
- up_grad: float32 [2048, 4096], P('fs', 'tp')
- down_grad: float32 [4096, 2048], P('tp', 'fs')
All inputs are finite; a program needn't handle non-finite values.
Results may differ from a plain program's by a relative error of at most 0.013.
Values may be sent and summed in bfloat16 or wider, within the bound.
A program may use at most 128 MiB of HBM per device.

v0:
```python
import functools
import math

import jax
import jax.numpy as jnp
from jax import lax
from jax.experimental import pallas as pl
from jax.experimental.pallas import tpu as pltpu
from jax.sharding import PartitionSpec as P

MESH = pl.DeviceIdType.MESH
CHUNKS = 2
BF16, F32 = jnp.bfloat16, jnp.float32
NT = (((1,), (1,)), ((), ()))


def ring_place(f, n):
    odd = lax.rem(f, 2)
    half = lax.div(f, 2)
    return half * (1 - odd) + (n - 1 - half) * odd


def ring_member(p, n):
    back = lax.div(p, (n + 1) // 2)
    return 2 * p * (1 - back) + (2 * n - 1 - 2 * p) * back


def tile_of(size, most):
    while size % most:
        most //= 2
    return most


def kernel(
    R, n, T,
    x_ref, c_ref, u_ref, d_ref,
    ig_ref, gu_ref, gd_ref,
    xg, cg, xt, ug, dg, pre, agr, pg, at,
    igp, itr, isum, irr, us, ur, ds_, dr_, fu, fd, fur, fdr,
    ag_ss, ag_rs, rs_ss, rs_rs, tr_ss, tr_rs, tt_ss, tt_rs,
    it_ss, it_rs, ir_ss, ir_rs, f_ss, f_rs,
):
    r, f, t = lax.axis_index("rep"), lax.axis_index("fs"), lax.axis_index("tp")
    tok, db = x_ref.shape[0], u_ref.shape[0]
    C, w = pre.shape[0], pre.shape[2]
    hb = C * w
    rows = R * T * tok

    def hidden(place, ch):
        return pl.ds(pl.multiple_of(place * hb + ch * w, w), w)

    for ref, full in ((x_ref, xg), (c_ref, cg)):
        for q in range(n):
            full[q, 0:tok, :] = ref[:, q * db:(q + 1) * db]
    p = ring_place(f, n)

    def member(q):
        return ring_member(lax.rem(p + q + n, n), n)

    def ring_dev(sign):
        return (r, member(sign), t)

    def rep_dev(q):
        return (lax.rem(r + q + R, R), f, t)

    def tp_dev(q):
        return (r, f, lax.rem(t + q + T, T))

    barrier = pltpu.get_barrier_semaphore()
    peers = [ring_dev(1), ring_dev(-1)]
    peers += [rep_dev(q) for q in range(1, R)] + [tp_dev(q) for q in range(1, T)]
    for peer in peers:
        pl.semaphore_signal(barrier, inc=1, device_id=peer, device_id_type=MESH)
    pl.semaphore_wait(barrier, len(peers))

    def remote(src, dst, ssem, rsem, dev):
        return pltpu.make_async_remote_copy(
            src_ref=src, dst_ref=dst, send_sem=ssem, recv_sem=rsem,
            device_id=dev, device_id_type=MESH,
        )

    long, short = n // 2, (n - 1) // 2
    streams = [(0, 1, long), (0, -1, short), (1, 1, short), (1, -1, long)]
    hops = max(long, short)
    def own(g, ch):
        return u_ref.at[:, hidden(r, ch)] if g == 0 else d_ref.at[hidden(r, ch), :]

    held = (ug, dg)

    def slot(sign, s):
        return (n - s if sign > 0 else s) - 1

    def gather_copy(ch, i, s):
        g, sign, _ = streams[i]
        src = own(g, ch) if s == 1 else held[g].at[slot(sign, s - 1), ch]
        return remote(
            src, held[g].at[slot(sign, s), ch],
            ag_ss.at[ch, i, s - 1], ag_rs.at[ch, i, s - 1], ring_dev(sign),
        )

    sends = []

    def go(copy):
        copy.start()
        sends.append(copy)
        return copy

    flying = {}

    def gather_first(ch):
        for i, (g, sign, k) in enumerate(streams):
            if k >= 1:
                flying[ch, i, 1] = go(gather_copy(ch, i, 1))

    gather_first(0)

    tokens = tuple((full.at[:, 0:tok, :], full) for full in (xg, cg))

    def span(dt, dr):
        return pl.ds((dt * R + dr) * tok, tok)

    rep_copies = {}
    for dr in range(1, R):
        for j, (ref, full) in enumerate(tokens):
            rep_copies[j, dr] = go(remote(
                ref, full.at[:, span(0, dr), :], tr_ss.at[j, dr], tr_rs.at[j, dr], rep_dev(-dr)
            ))
    tp_copies = {}
    for dt in range(1, T):
        for j, (ref, full) in enumerate(tokens):
            tp_copies[j, dt, 0] = go(remote(
                ref, full.at[:, span(dt, 0), :], tt_ss.at[j, dt, 0], tt_rs.at[j, dt, 0],
                tp_dev(-dt),
            ))

    row_tile = tile_of(rows, 256)

    def gather_dot(ch, g, block, q, first=False):
        b = member(q)
        out, full = ((pre, xg), (agr, cg))[g]

        @pl.loop(0, rows // row_tile)
        def _(i):
            part = pl.ds(pl.multiple_of(i * row_tile, row_tile), row_tile)
            lhs = full[b, part, :]
            if g == 0:
                val = jnp.dot(lhs, block[...], preferred_element_type=F32)
            else:
                val = lax.dot_general(lhs, block[...], NT, preferred_element_type=F32)
            if first:
                out[ch, part, :] = val
            else:
                out[ch, part, :] += val

    def finish_tokens():
        for dr in range(1, R):
            for j, (ref, full) in enumerate(tokens):
                rep_copies[j, dr].wait_recv()
                for dt in range(1, T):
                    tp_copies[j, dt, dr] = go(remote(
                        full.at[:, span(0, dr), :], full.at[:, span(dt, dr), :],
                        tt_ss.at[j, dt, dr], tt_rs.at[j, dt, dr], tp_dev(-dt),
                    ))
        for copy in tp_copies.values():
            copy.wait_recv()

        @pl.loop(0, n)
        def _(b):
            xt[b] = xg[b].T

        for ch in range(C):
            gather_dot(ch, 0, own(0, ch), 0, True)
            gather_dot(ch, 1, own(1, ch), 0, True)

    act_tile = tile_of(rows, 128)

    def activate(ch):
        @pl.loop(0, rows // act_tile)
        def _(i):
            part = pl.ds(pl.multiple_of(i * act_tile, act_tile), act_tile)
            active = jnp.maximum(pre[ch, part, :], 0.0)
            pg[ch, part, :] = (2.0 * active * agr[ch, part, :]).astype(BF16)
            at[ch, :, part] = (active * active).astype(BF16).T

    def gather(ch, before_last):
        for s in range(1, hops + 1):
            if s == hops:
                before_last()
            for i, (g, sign, k) in enumerate(streams):
                if s <= k:
                    flying[ch, i, s].wait_recv()
                    if s < k:
                        flying[ch, i, s + 1] = go(gather_copy(ch, i, s + 1))
            if s == 1 and ch == 0:
                finish_tokens()
            for i, (g, sign, k) in enumerate(streams):
                if s <= k:
                    gather_dot(ch, g, held[g].at[slot(sign, s), ch], -sign * s)
        if hops == 0:
            if ch == 0:
                finish_tokens()
            before_last()
        activate(ch)

    def grad_block(ch, g, q, dst, arrived):
        b = member(q)
        height = (db, w)[g]
        tile = tile_of(height, 256)

        @pl.loop(0, height // tile)
        def _(i):
            part = pl.ds(pl.multiple_of(i * tile, tile), tile)
            if g == 0:
                val = jnp.dot(xt[b, part, :], pg[ch], preferred_element_type=F32)
            else:
                val = jnp.dot(at[ch, part, :], cg[b], preferred_element_type=F32)
            for a in arrived:
                val = val + a[part, :].astype(F32)
            dst[part, :] = val.astype(BF16)

    rs_send, rs_recv = (us, ds_), (ur, dr_)

    def rs_index(i, s):
        g, sign, _ = streams[i]
        return s - 1 if sign > 0 else (long, short)[g] + s - 1

    reducing = {}

    def reduce_step(ch, i, s):
        g, sign, k = streams[i]
        arrived = []
        if s > 1:
            reducing[ch, i, s - 1].wait_recv()
            arrived = [rs_recv[g].at[rs_index(i, s - 1), ch]]
        mine = rs_send[g].at[rs_index(i, s), ch]
        grad_block(ch, g, sign * (k - s + 1), mine, arrived)
        reducing[ch, i, s] = go(remote(
            mine, rs_recv[g].at[rs_index(i, s), ch],
            rs_ss.at[ch, i, s - 1], rs_rs.at[ch, i, s - 1], ring_dev(sign),
        ))

    def reduce_all(ch, s):
        for i, (g, sign, k) in enumerate(streams):
            if s <= k:
                reduce_step(ch, i, s)

    for ch in range(C):
        if ch + 1 < C:
            gather(ch, functools.partial(gather_first, ch + 1))
        elif C > 1:
            gather(ch, functools.partial(reduce_all, 0, 1))
        else:
            gather(ch, lambda: None)
            reduce_all(ch, 1)

    for q in range(n):
        b = member(q)

        @pl.loop(0, rows // row_tile)
        def _(i):
            part = pl.ds(pl.multiple_of(i * row_tile, row_tile), row_tile)
            val = 0.0
            for ch in range(C):
                block = own(0, ch) if q == 0 else ug.at[q - 1, ch]
                val = val + lax.dot_general(
                    pg[ch, part, :], block[...], NT, preferred_element_type=F32
                )
            igp[b, part, :] = val.astype(BF16)

    wide = R * tok
    it_copies = [
        go(remote(
            igp.at[:, pl.ds(dt * wide, wide), :], itr.at[dt - 1],
            it_ss.at[dt], it_rs.at[dt], tp_dev(dt),
        ))
        for dt in range(1, T)
    ]
    ir_copies = []

    def finish_tp():
        for copy in it_copies:
            copy.wait_recv()

        @pl.loop(0, n)
        def _(b):
            for dr in range(R):
                part = pl.ds(dr * tok, tok)
                val = igp[b, part, :].astype(F32)
                for dt in range(1, T):
                    val = val + itr[dt - 1, b, part, :].astype(F32)
                isum[dr, b] = val.astype(BF16)

        for dr in range(1, R):
            ir_copies.append(go(remote(
                isum.at[dr], irr.at[dr - 1], ir_ss.at[dr], ir_rs.at[dr], rep_dev(dr)
            )))

    def finish_rep():
        for copy in ir_copies:
            copy.wait_recv()

        for b in range(n):
            val = isum[0, b].astype(F32)
            for dr in range(1, R):
                val = val + irr[dr - 1, b].astype(F32)
            ig_ref[:, b * db:(b + 1) * db] = val.astype(BF16)

    finish_tp()

    finals = ((fu, fur, gu_ref), (fd, fdr, gd_ref))
    fin_copies = {}

    def put(g, place, ch, val):
        if g == 0:
            gu_ref[:, hidden(place, ch)] = val
        else:
            gd_ref[hidden(place, ch), :] = val

    def finish(ch, g):
        mine, theirs, out = finals[g]
        arrived = []
        for i, (h, sign, k) in enumerate(streams):
            if h == g and k >= 1:
                reducing[ch, i, k].wait_recv()
                arrived.append(rs_recv[g].at[rs_index(i, k), ch])
        grad_block(ch, g, 0, mine.at[ch], arrived)
        for dr in range(1, R):
            fin_copies[ch, g, dr] = go(remote(
                mine.at[ch], theirs.at[dr - 1, ch],
                f_ss.at[ch, g, dr], f_rs.at[ch, g, dr], rep_dev(-dr),
            ))
        put(g, r, ch, mine[ch])

    for ch in range(C):
        for s in range(2, hops + 1):
            reduce_all(ch, s)
            if ch == 0 and s == 2:
                finish_rep()
        if ch == 0 and hops < 2:
            finish_rep()
        if ch + 1 < C:
            reduce_all(ch + 1, 1)
        for g in range(2):
            finish(ch, g)
    for (ch, g, dr), copy in fin_copies.items():
        _, theirs, out = finals[g]
        copy.wait_recv()
        put(g, lax.rem(r + dr, R), ch, theirs[dr - 1, ch])
    for copy in sends:
        copy.wait_send()


def shards(inputs, cotangent, up_weight, down_weight):
    R, n, T = lax.axis_size("rep"), lax.axis_size("fs"), lax.axis_size("tp")
    tok, D = inputs.shape
    db, hb = up_weight.shape[0], up_weight.shape[1] // R
    rows = R * T * tok
    C = tile_of(hb // 128, CHUNKS) if hb > 128 else 1
    w = hb // C
    V, S = pltpu.VMEM, pltpu.SemaphoreType.DMA
    hops = max(n // 2, 1)
    m = max(n - 1, 1)
    scratch = [
        V((n, rows, db), BF16), V((n, rows, db), BF16), V((n, db, rows), BF16),
        V((m, C, db, w), BF16), V((m, C, w, db), BF16),
        V((C, rows, w), F32), V((C, rows, w), F32), V((C, rows, w), BF16), V((C, w, rows), BF16),
        V((n, rows, db), BF16), V((max(T - 1, 1), n, R * tok, db), BF16),
        V((R, n, tok, db), BF16), V((max(R - 1, 1), n, tok, db), BF16),
        V((m, C, db, w), BF16), V((m, C, db, w), BF16),
        V((m, C, w, db), BF16), V((m, C, w, db), BF16),
        V((C, db, w), BF16), V((C, w, db), BF16),
        V((max(R - 1, 1), C, db, w), BF16), V((max(R - 1, 1), C, w, db), BF16),
        S((C, 4, hops)), S((C, 4, hops)), S((C, 4, hops)), S((C, 4, hops)),
        S((2, R)), S((2, R)), S((2, T, R)), S((2, T, R)),
        S((T,)), S((T,)), S((R,)), S((R,)), S((C, 2, R)), S((C, 2, R)),
    ]
    vmem = pl.BlockSpec(memory_space=pltpu.VMEM)
    ig, gu, gd = pl.pallas_call(
        functools.partial(kernel, R, n, T),
        out_shape=(
            jax.ShapeDtypeStruct((tok, D), BF16),
            jax.ShapeDtypeStruct((db, R * hb), BF16),
            jax.ShapeDtypeStruct((R * hb, db), BF16),
        ),
        in_specs=[vmem] * 4,
        out_specs=(vmem,) * 3,
        scratch_shapes=scratch,
        compiler_params=pltpu.CompilerParams(
            collective_id=0, has_side_effects=True, vmem_limit_bytes=60 * 2**20
        ),
    )(inputs, cotangent, up_weight, down_weight)
    total_tokens = tok * R * n * T
    loss_scale = 1.0 / math.sqrt(total_tokens)
    return ig, gu.astype(F32) * loss_scale, gd.astype(F32) * loss_scale


def solution(mesh):
    token, up, down = P(("rep", "fs", "tp"), None), P("fs", "tp"), P("tp", "fs")
    return jax.shard_map(
        shards,
        mesh=mesh,
        in_specs=(token, token, up, down),
        out_specs=(token, up, down),
        check_vma=False,
    )
```

profile of v0, /device:TPU:0, one launch (start us, length us, event | category | flops | bytes accessed | tf_op | source)
XLA Modules:
  0.0 201.8 jit_solution(6366145026224585925)
XLA Ops:
  0.6 196.0 %shard_map.67 = (bf16[128,2048]{1,0:T(8,128)(2,1)}, bf16[256,2048]{1,0:T(8,128)(2,1)}, bf16[2048,256]{1,0:T(8,128)(2,1)}) custom-call(bf16[128,2048]{1,0:T(8,128)(2,1)} %x_ref.1, bf16[128,2048]{1,0:T(8,128)(2,1)} %c_ref.1, bf16[256,2048]{1,0:T(8,128)(2,1)} %u_ref.1, bf16[2048,256]{1,0:T(8,128)(2,1)} %d_ref.1), custom_call_target="tpu_custom_call" | custom-call | tf_op jit(solution)/shard_map/pallas_call | solution.py:378
  196.7 0.0 copy-start
  196.7 2.9 %convert_multiply_fusion.1 = f32[256,2048]{1,0:T(8,128)} fusion(bf16[256,2048]{1,0:T(8,128)(2,1)} %get-tuple-element.7), kind=kLoop, calls=%fused_computation.1 | loop fusion | flops 1048576 | bytes 3145728 | tf_op jit(solution)/shard_map/mul | solution.py:394
  199.6 0.0 copy-done
  199.6 0.0 copy-start.1
  199.6 1.5 convert_multiply_fusion
  201.0 0.0 copy-done.1
  201.0 0.8 copy.8
Async XLA Ops:
  196.7 2.9 %copy-start = (bf16[2048,256]{1,0:T(8,128)(2,1)S(1)}, bf16[2048,256]{1,0:T(8,128)(2,1)}, u32[]{:S(2)}) copy-start(bf16[2048,256]{1,0:T(8,128)(2,1)} %get-tuple-element.8) | copy-start | bytes 3145732
  199.6 1.5 copy-start.1
where the time goes:
time: 202 us
  Pallas kernels  196 us (97%)
  other arithmetic  4.33 us (2%)
    pallas_call x1, Pallas kernels, shards(): pl.pallas_call(functools.partial(kernel, R, n, T), out_shape=(jax.ShapeDt...  196 us
    mul x2, other arithmetic, shards(): return (ig, gu.astype(F32) * loss_scale, gd.astype(F32) * loss_scale)  4.33 us

commit v1 on v0

--- a/solution.py
+++ b/solution.py
@@ -31,7 +31,7 @@
     return most
 
 
-def kernel(
+def ring_kernel(
     R, n, T,
     x_ref, c_ref, u_ref, d_ref,
     ig_ref, gu_ref, gd_ref,
@@ -350,8 +350,517 @@
         copy.wait_send()
 
 
-def shards(inputs, cotangent, up_weight, down_weight):
-    R, n, T = lax.axis_size("rep"), lax.axis_size("fs"), lax.axis_size("tp")
+def plane_kernel(
+    Z,
+    x_ref, c_ref, u_ref, d_ref,
+    ig_ref, gu_ref, gd_ref,
+    xg, cg, xt, ug, dg, pre, pg, at,
+    igp, itr, isum, ira, irb, ipt, ift, su, sd, ru, rd, fu, fd,
+    yw_s, yw_r, zg_s, zg_r, tx_s, tx_r, ty_s, ty_r, tt_s, tt_r,
+    rs_s, rs_r, fy_s, fy_r, fx_s, fx_r, ig_s, ig_r,
+):
+    r, f, t = lax.axis_index("rep"), lax.axis_index("fs"), lax.axis_index("tp")
+    z, y = lax.div(f, 2), lax.rem(f, 2)
+    tok, D = x_ref.shape
+    db = u_ref.shape[0]
+    C, hc = pg.shape[0], pg.shape[2]
+    hw, half, wide = C * hc, tok // 2, 2 * tok
+    n = 2 * Z
+    xdev, ydev, tdev = (1 - r, f, t), (r, f + 1 - 2 * y, t), (r, f, 1 - t)
+
+    def zdev(s):
+        return (r, f + 2 * s, t)
+
+    low = z < Z // 2
+    m = jnp.where(low, z, Z - 1 - z)
+    near = (jnp.where(low, 0, 1), jnp.where(low, 1, -1))
+    far = (1 - near[0], -near[1])
+
+    barrier = pltpu.get_barrier_semaphore()
+
+    def greet(dev):
+        pl.semaphore_signal(barrier, inc=1, device_id=dev, device_id_type=MESH)
+
+    for dev in (xdev, ydev, tdev):
+        greet(dev)
+    ahead = {1: z < Z - 1, -1: z > 0}
+    for s in (1, -1):
+        pl.when(ahead[s])(functools.partial(greet, zdev(s)))
+    pl.semaphore_wait(barrier, 3 + sum(jnp.where(ahead[s], 1, 0) for s in (1, -1)))
+
+    sends = []
+
+    def remote(src, dst, ssem, rsem, dev):
+        return pltpu.make_async_remote_copy(
+            src_ref=src, dst_ref=dst, send_sem=ssem, recv_sem=rsem,
+            device_id=dev, device_id_type=MESH,
+        )
+
+    def go(make, cond=None):
+        make().start()
+        sends.append((cond, make))
+
+    def span(at_, size):
+        return pl.ds(pl.multiple_of(at_, size), size)
+
+    def blk(b):
+        return span(b * db, db)
+
+    def hid(q, ch):
+        return span(q * hw + ch * hc, hc)
+
+    mine, other = 2 * r + y, 2 * r + 1 - y
+
+    def own(g, q, ch):
+        return u_ref.at[:, hid(q, ch)] if g == 0 else d_ref.at[hid(q, ch), :]
+
+    def held(g, ch, b):
+        return ug.at[ch, blk(b), :] if g == 0 else dg.at[ch, :, blk(b)]
+
+    def swap(ch, g):
+        return remote(own(g, other, ch), held(g, ch, f), yw_s.at[ch, g], yw_r.at[ch, g], ydev)
+
+    def origin(s, k, e):
+        return f - 2 * s * k + e * (1 - 2 * y)
+
+    def pass_on(ch, g, s, k, e):
+        block = held(g, ch, origin(s, k, e))
+        src = own(g, mine, ch) if k == 0 and e == 0 else block
+        i = (ch, (1 - s) // 2, k, e, g)
+        return remote(src, block, zg_s.at[i], zg_r.at[i], zdev(s))
+
+    def landed(ch, g, s, k, e):
+        block = held(g, ch, origin(s, k, e))
+        i = (ch, (1 - s) // 2, k - 1, e, g)
+        return remote(block, block, zg_s.at[i], zg_r.at[i], zdev(s))
+
+    def begin(ch, g, e, also=None):
+        for s in (1, -1):
+            cond = ahead[s] if also is None else ahead[s] & also
+            pl.when(cond)(functools.partial(
+                go, functools.partial(pass_on, ch, g, s, 0, e), cond))
+
+    level = [m == m0 for m0 in range(Z // 2)]
+    reached = {}
+    for k in range(1, Z):
+        reached[1, k], reached[-1, k] = z >= k, z < Z - k
+    passing = {key: reached[key] & ahead[key[0]] for key in reached}
+
+    def relay(ch, g, k):
+        for e in range(2):
+            for s in (1, -1):
+                cond = passing[s, k]
+
+                @pl.when(cond)
+                def _():
+                    landed(ch, g, s, k, e).wait_recv()
+                    go(functools.partial(pass_on, ch, g, s, k, e), cond)
+
+    def collect(ch, g):
+        for k in range(1, Z):
+            for e in range(2):
+                for s in (1, -1):
+
+                    @pl.when(reached[s, k] & jnp.logical_not(ahead[s]))
+                    def _():
+                        landed(ch, g, s, k, e).wait_recv()
+
+    def swapped(ch, g, also=None):
+        begin(ch, g, 1, also)
+
+    def rows(k, dt, part=(0, 2)):
+        lo, hi = part
+        return pl.ds((2 * k + dt) * tok + lo * half, (hi - lo) * half)
+
+    def quarter(i):
+        return span(jnp.where(low, Z - 1 - i, i) * 2 * db, 2 * db)
+
+    A, B, AB = (0, 1), (1, 2), (0, 2)
+
+    def hop(sems, i, dev, full, src, dst, cols, ref=None):
+        def make():
+            where = slice(None) if cols is None else quarter(cols)
+            if ref is None:
+                take = full.at[rows(*src), where]
+            else:
+                take = ref.at[pl.ds(src[2][0] * half, (src[2][1] - src[2][0]) * half), where]
+            return remote(
+                take, full.at[rows(*dst), where], sems[0].at[i], sems[1].at[i], dev
+            )
+
+        return make
+
+    X, Y, S = (tx_s, tx_r), (ty_s, ty_r), (tt_s, tt_r)
+    moves = {}
+    for i, part in enumerate((A, B)):
+        moves["x", "x", i] = hop(X, i, xdev, xg, (0, 0, part), (1, 0, part), None, x_ref)
+        moves["y", "x", i] = hop(Y, i, ydev, xg, (0, 0, part), (2, 0, part), None, x_ref)
+        moves["d", "x", i] = hop(X, 2 + i, xdev, xg, (2, 0, part), (3, 0, part), None)
+    moves["s", "x", 0] = hop(S, 0, tdev, xg, (0, 0, AB), (0, 1, AB), None, x_ref)
+    moves["s", "c", 0] = hop(S, 1, tdev, cg, (0, 0, AB), (0, 1, AB), None, c_ref)
+    for k in range(1, 4):
+        moves["s", "x", k] = hop(S, 1 + k, tdev, xg, (k, 0, AB), (k, 1, AB), None)
+    for i in range(Z):
+        moves["x", "c", i] = hop(X, 4 + 2 * i, xdev, cg, (0, 0, AB), (1, 0, AB), i, c_ref)
+        moves["y", "c", i] = hop(Y, 2 + 2 * i, ydev, cg, (0, 0, AB), (2, 0, AB), i, c_ref)
+        moves["dx", "c", i] = hop(X, 5 + 2 * i, xdev, cg, (2, 0, A), (3, 0, A), i)
+        moves["dy", "c", i] = hop(Y, 3 + 2 * i, ydev, cg, (1, 0, B), (3, 0, B), i)
+        for k in range(1, 4):
+            moves["s%d" % k, "c", i] = hop(
+                S, 5 + (k - 1) * Z + i, tdev, cg, (k, 0, AB), (k, 1, AB), i)
+
+    def start(*key):
+        go(moves[key])
+
+    def arrive(*key):
+        moves[key]().wait_recv()
+
+    def flip(k):
+        part = pl.ds(k * wide, wide)
+
+        @pl.loop(0, n)
+        def _(b):
+            xt[blk(b), part] = xg[part, blk(b)].T
+
+    def forward(ch, first, last):
+        @pl.loop(first, last)
+        def _(k):
+            part = span(k * wide, wide)
+            active = jnp.maximum(
+                jnp.dot(xg[part, :], ug[ch], preferred_element_type=F32), 0.0)
+            pre[ch, part, :] = active
+            at[ch, :, part] = (active * active).astype(BF16).T
+
+    def backward(ch):
+        @pl.loop(0, 4)
+        def _(k):
+            part = span(k * wide, wide)
+            val = lax.dot_general(cg[part, :], dg[ch], NT, preferred_element_type=F32)
+            pg[ch, part, :] = (2.0 * pre[ch, part, :] * val).astype(BF16)
+
+    def grad(ch, g, b):
+        if g == 0:
+            return jnp.dot(xt[blk(b), :], pg[ch], preferred_element_type=F32)
+        return jnp.dot(at[ch], cg[:, blk(b)], preferred_element_type=F32)
+
+    out_buf, in_buf, fin = (su, sd), (ru, rd), (fu, fd)
+
+    def partial_copy(ch, g, way, j):
+        d, s = way
+        return remote(
+            out_buf[g].at[d, j, ch], in_buf[g].at[d, j, ch],
+            rs_s.at[d, j, ch, g], rs_r.at[d, j, ch, g], zdev(s))
+
+    def reduce(ch, g, way, j, m0):
+        cond = level[m0]
+        to = jnp.where(way[1] > 0, Z - 1 - j, j)
+        make = functools.partial(partial_copy, ch, g, way, j)
+        more = m0 > 0 or way is far
+        if more:
+            make().wait_recv()
+
+        @pl.loop(0, 2)
+        def _(h):
+            val = grad(ch, g, 2 * to + h)
+            if more:
+                val = val + in_buf[g][way[0], j, ch, h].astype(F32)
+            out_buf[g][way[0], j, ch, h] = val.astype(BF16)
+
+        go(make, cond)
+
+    def place(g, q, ch):
+        return gu_ref.at[:, hid(q, ch)] if g == 0 else gd_ref.at[hid(q, ch), :]
+
+    def final_y(ch, g):
+        return remote(
+            fin[g].at[ch, 1 - y], place(g, mine, ch), fy_s.at[ch, g], fy_r.at[ch, g], ydev)
+
+    def final_y_in(ch, g):
+        return remote(
+            place(g, other, ch), place(g, other, ch), fy_s.at[ch, g], fy_r.at[ch, g], ydev)
+
+    def final_x(ch, g, e):
+        src = fin[g].at[ch, y] if e == 0 else place(g, other, ch)
+        q = other if e else mine
+        i = (ch, g, e)
+        return remote(src, place(g, q, ch), fx_s.at[i], fx_r.at[i], xdev)
+
+    def final_x_in(ch, g, e):
+        q = 2 * (1 - r) + (1 - y if e else y)
+        i = (ch, g, e)
+        return remote(place(g, q, ch), place(g, q, ch), fx_s.at[i], fx_r.at[i], xdev)
+
+    def finish(ch, g, m0):
+        cond = level[m0]
+        ways = [(far, m0)] + ([(near, Z - 1 - m0)] if m0 else [])
+        for way, j in ways:
+            partial_copy(ch, g, way, j).wait_recv()
+
+        @pl.loop(0, 2)
+        def _(h):
+            val = grad(ch, g, 2 * z + h)
+            for way, j in ways:
+                val = val + in_buf[g][way[0], j, ch, h].astype(F32)
+            fin[g][ch, h] = val.astype(BF16)
+
+        go(functools.partial(final_y, ch, g), cond)
+        go(functools.partial(final_x, ch, g, 0), cond)
+        if g == 0:
+            gu_ref[:, hid(mine, ch)] = fu[ch, y]
+        else:
+            gd_ref[hid(mine, ch), :] = fd[ch, y]
+
+    def spread(ch, g, m0):
+        final_y_in(ch, g).wait_recv()
+        go(functools.partial(final_x, ch, g, 1), level[m0])
+
+    hd = D // 2
+
+    def ig_copy(i):
+        if i == 0:
+            return remote(igp.at[:, pl.ds(tok, tok), :], itr, ig_s.at[0], ig_r.at[0], tdev)
+        side, step = (i - 1) % 2, (i - 1) // 2
+        if step < 2:
+            src = isum.at[side, 3 if step else 1 + side]
+            dst = (ira, irb)[side].at[step]
+        else:
+            src, dst = ipt.at[side], ift.at[side]
+        dev = (xdev, ydev)[side if step < 2 else 1 - side]
+        return remote(src, dst, ig_s.at[i], ig_r.at[i], dev)
+
+    def ig_go(i, cond):
+        go(functools.partial(ig_copy, i), cond)
+
+    def ig_partial(cond):
+        @pl.loop(0, 4)
+        def _(k):
+            part = span(k * wide, wide)
+
+            @pl.loop(0, n)
+            def _(b):
+                val = 0.0
+                for ch in range(C):
+                    val = val + lax.dot_general(
+                        pg[ch, part, :], ug[ch, blk(b), :], NT, preferred_element_type=F32)
+                igp[k, :, blk(b)] = val.astype(BF16)
+
+        ig_go(0, cond)
+
+    def ig_first(cond):
+        ig_copy(0).wait_recv()
+
+        @pl.loop(0, 4)
+        def _(k):
+            for side in range(2):
+                cols = pl.ds(side * hd, hd)
+                val = igp[k, 0:tok, cols].astype(F32) + itr[k, :, cols].astype(F32)
+                isum[side, k] = val.astype(BF16)
+
+        for i in range(1, 5):
+            ig_go(i, cond)
+
+    def ig_second(cond):
+        for i in range(1, 5):
+            ig_copy(i).wait_recv()
+        for side, got in enumerate((ira, irb)):
+            val = isum[side, 2 - side].astype(F32) + got[1].astype(F32)
+            ipt[side] = val.astype(BF16)
+            ig_go(5 + side, cond)
+
+    def ig_last():
+        for side, got in enumerate((ira, irb)):
+            ig_copy(5 + side).wait_recv()
+            val = isum[side, 0].astype(F32) + got[0].astype(F32) + ift[side].astype(F32)
+            ig_ref[:, side * hd:(side + 1) * hd] = val.astype(BF16)
+
+    edge, inner = level[0], m > 0
+    last = C - 1
+
+    begin(0, 0, 0)
+    go(functools.partial(swap, 0, 0))
+    for i in range(2):
+        start("x", "x", i)
+        start("y", "x", i)
+    begin(0, 1, 0, edge)
+    start("s", "x", 0)
+    start("s", "c", 0)
+    for ch in range(C):
+        for g in range(2):
+            if ch or g:
+                go(functools.partial(swap, ch, g))
+    xg[0:tok, :] = x_ref[...]
+    cg[0:tok, :] = c_ref[...]
+    for ch in range(C):
+        ug[ch, blk(f), :] = u_ref[:, hid(mine, ch)]
+        dg[ch, :, blk(f)] = d_ref[hid(mine, ch), :]
+
+    swap(0, 0).wait_recv()
+    begin(0, 0, 1)
+    for ch in range(1, C):
+        for g in range(2):
+            begin(ch, g, 0, edge)
+    relay(0, 0, 1)
+    arrive("s", "x", 0)
+    arrive("s", "c", 0)
+    flip(0)
+    arrive("y", "x", 0)
+    start("d", "x", 0)
+    for k in range(2, Z - 1):
+        relay(0, 0, k)
+    begin(0, 1, 0, inner)
+    for i in range(2):
+        arrive("x", "x", i)
+    start("s", "x", 1)
+    arrive("y", "x", 1)
+    start("d", "x", 1)
+    start("x", "c", 0)
+    start("y", "c", 0)
+    start("s", "x", 2)
+    swap(0, 1).wait_recv()
+    begin(0, 1, 1)
+    arrive("s", "x", 1)
+    flip(1)
+    arrive("s", "x", 2)
+    flip(2)
+    relay(0, 1, 1)
+    collect(0, 0)
+    forward(0, 0, 3)
+    for ch in range(1, C):
+        for g in range(2):
+            swap(ch, g).wait_recv()
+            begin(ch, g, 1, edge)
+    for i in range(2):
+        arrive("d", "x", i)
+    start("s", "x", 3)
+    for k in range(2, Z - 1):
+        relay(0, 1, k)
+    for ch in range(1, C):
+        begin(ch, 0, 0, inner)
+        begin(ch, 0, 1, inner)
+    arrive("s", "x", 3)
+    flip(3)
+    forward(0, 3, 4)
+    for i in range(Z):
+        if i + 1 < Z:
+            start("x", "c", i + 1)
+            start("y", "c", i + 1)
+        arrive("x", "c", i)
+        start("dy", "c", i)
+        start("s1", "c", i)
+        arrive("y", "c", i)
+        start("dx", "c", i)
+        start("s2", "c", i)
+        if 1 <= i < Z - 1:
+            for ch in range(1, C):
+                relay(ch, 0, i)
+                if i == Z - 2:
+                    begin(ch, 1, 0, inner)
+                    begin(ch, 1, 1, inner)
+        arrive("dy", "c", i)
+        arrive("dx", "c", i)
+        start("s3", "c", i)
+        for k in range(1, 4):
+            arrive("s%d" % k, "c", i)
+        if i < Z - 1:
+            pl.when(edge)(functools.partial(reduce, 0, 1, near, i, 0))
+    collect(0, 1)
+    backward(0)
+
+    def edges():
+        for j in range(Z - 1):
+            reduce(0, 0, near, j, 0)
+        for ch in range(1, C):
+            collect(ch, 0)
+            forward(ch, 0, 4)
+            for j in range(Z - 1):
+                reduce(ch, 1, near, j, 0)
+            collect(ch, 1)
+            backward(ch)
+            for j in range(Z - 1):
+                reduce(ch, 0, near, j, 0)
+        ig_partial(edge)
+        finish(0, 1, 0)
+        ig_first(edge)
+        spread(0, 1, 0)
+        finish(0, 0, 0)
+        ig_second(edge)
+        spread(0, 0, 0)
+        for ch in range(1, C):
+            finish(ch, 1, 0)
+            if ch == 1:
+                ig_last()
+            spread(ch, 1, 0)
+            finish(ch, 0, 0)
+            spread(ch, 0, 0)
+
+    def inside(m0):
+        cond = level[m0]
+
+        def some(ch, g):
+            for j in range(Z - 1 - m0):
+                reduce(ch, g, near, j, m0)
+                if j < m0:
+                    reduce(ch, g, far, j, m0)
+
+        for j in range(Z - 1 - m0):
+            reduce(0, 1, near, j, m0)
+            if j + 1 < Z - 1:
+                for ch in range(1, C):
+                    relay(ch, 1, j + 1)
+        for ch in range(1, C):
+            for k in range(Z - m0, Z - 1):
+                relay(ch, 1, k)
+        for j in range(m0):
+            reduce(0, 1, far, j, m0)
+        for ch in range(1, C):
+            forward(ch, 0, 4)
+            backward(ch)
+        ig_partial(cond)
+        reduce(0, 0, near, 0, m0)
+        ig_first(cond)
+        finish(0, 1, m0)
+        for j in range(1, Z - 1 - m0):
+            reduce(0, 0, near, j, m0)
+        spread(0, 1, m0)
+        for j in range(m0):
+            reduce(0, 0, far, j, m0)
+        ig_second(cond)
+        finish(0, 0, m0)
+        for ch in range(1, C):
+            reduce(ch, 1, near, 0, m0)
+            if ch == 1:
+                spread(0, 0, m0)
+                ig_last()
+            for j in range(1, Z - 1 - m0):
+                reduce(ch, 1, near, j, m0)
+            for j in range(m0):
+                reduce(ch, 1, far, j, m0)
+            finish(ch, 1, m0)
+            reduce(ch, 0, near, 0, m0)
+            spread(ch, 1, m0)
+            for j in range(1, Z - 1 - m0):
+                reduce(ch, 0, near, j, m0)
+            for j in range(m0):
+                reduce(ch, 0, far, j, m0)
+            finish(ch, 0, m0)
+            spread(ch, 0, m0)
+
+    pl.when(edge)(edges)
+    for m0 in range(1, Z // 2):
+        pl.when(level[m0])(functools.partial(inside, m0))
+    for ch in range(C):
+        for g in (1, 0):
+            for e in range(2):
+                final_x_in(ch, g, e).wait_recv()
+    for cond, make in sends:
+        if cond is None:
+            make().wait_send()
+        else:
+            pl.when(cond)(lambda: make().wait_send())
+
+
+def ring_call(inputs, up_weight):
+    R, n, T = axis_sizes()
     tok, D = inputs.shape
     db, hb = up_weight.shape[0], up_weight.shape[1] // R
     rows = R * T * tok
@@ -374,13 +883,58 @@
         S((2, R)), S((2, R)), S((2, T, R)), S((2, T, R)),
         S((T,)), S((T,)), S((R,)), S((R,)), S((C, 2, R)), S((C, 2, R)),
     ]
+    return functools.partial(ring_kernel, R, n, T), scratch, (R, hb)
+
+
+def axis_sizes():
+    return lax.axis_size("rep"), lax.axis_size("fs"), lax.axis_size("tp")
+
+
+def plane_call(inputs, up_weight):
+    R, n, T = axis_sizes()
+    tok, D = inputs.shape
+    db, HB = up_weight.shape
+    Z, G = n // 2, 2 * R
+    if R != 2 or T != 2 or n % 4 or tok % 32 or HB % (128 * G) or db % 128:
+        return None
+    hw = HB // G
+    C = tile_of(hw // 128, CHUNKS)
+    hc = hw // C
+    rows, hd = 8 * tok, D // 2
+    V, S = pltpu.VMEM, pltpu.SemaphoreType.DMA
+    data = [
+        ((rows, D), BF16), ((rows, D), BF16), ((D, rows), BF16),
+        ((C, D, hc), BF16), ((C, hc, D), BF16),
+        ((C, rows, hc), F32), ((C, rows, hc), BF16), ((C, hc, rows), BF16),
+        ((4, 2 * tok, D), BF16), ((4, tok, D), BF16), ((2, 4, tok, hd), BF16),
+        ((2, tok, hd), BF16), ((2, tok, hd), BF16), ((2, tok, hd), BF16), ((2, tok, hd), BF16),
+        ((2, Z - 1, C, 2, db, hc), BF16), ((2, Z - 1, C, 2, hc, db), BF16),
+        ((2, Z - 1, C, 2, db, hc), BF16), ((2, Z - 1, C, 2, hc, db), BF16),
+        ((C, 2, db, hc), BF16), ((C, 2, hc, db), BF16),
+    ]
+    size = sum(math.prod(s) * jnp.dtype(d).itemsize for s, d in data)
+    if size > 50 * 2**20:
+        return None
+    sems = [
+        (C, 2), (C, 2, Z - 1, 2, 2), (4 + 2 * Z,), (2 + 2 * Z,), (5 + 3 * Z,),
+        (2, Z - 1, C, 2), (C, 2), (C, 2, 2), (7,),
+    ]
+    scratch = [V(s, d) for s, d in data] + [S(s) for s in sems for _ in range(2)]
+    return functools.partial(plane_kernel, Z), scratch, (1, HB)
+
+
+def shards(inputs, cotangent, up_weight, down_weight):
+    R, n, T = axis_sizes()
+    tok, D = inputs.shape
+    db = up_weight.shape[0]
+    body, scratch, (parts, hb) = plane_call(inputs, up_weight) or ring_call(inputs, up_weight)
     vmem = pl.BlockSpec(memory_space=pltpu.VMEM)
     ig, gu, gd = pl.pallas_call(
-        functools.partial(kernel, R, n, T),
+        body,
         out_shape=(
             jax.ShapeDtypeStruct((tok, D), BF16),
-            jax.ShapeDtypeStruct((db, R * hb), BF16),
-            jax.ShapeDtypeStruct((R * hb, db), BF16),
+            jax.ShapeDtypeStruct((db, parts * hb), BF16),
+            jax.ShapeDtypeStruct((parts * hb, db), BF16),
         ),
         in_specs=[vmem] * 4,
         out_specs=(vmem,) * 3,

time: 202 us -> 162 us (0.80)
  Pallas kernels: 196 us -> 156 us
    pallas_call x1, Pallas kernels: 196 us -> 156 us  [shards(): pl.pallas_call(body, out_shape=(jax.ShapeDtypeStruct((tok, D), BF16), jax...]
where the time goes in v1:
time: 162 us
  Pallas kernels  156 us (96%)
  other arithmetic  4.33 us (3%)
    pallas_call x1, Pallas kernels, shards(): pl.pallas_call(body, out_shape=(jax.ShapeDtypeStruct((tok, D), BF16), jax...  156 us
    mul x2, other arithmetic, shards(): return (ig, gu.astype(F32) * loss_scale, gd.astype(F32) * loss_scale)  4.33 us

profile of v1, /device:TPU:0, one launch (start us, length us, event | category | flops | bytes accessed | tf_op | source)
XLA Modules:
  0.0 162.1 jit_solution(10491197929605603905)
XLA Ops:
  0.6 156.3 %shard_map.67 = (bf16[128,2048]{1,0:T(8,128)(2,1)}, bf16[256,2048]{1,0:T(8,128)(2,1)}, bf16[2048,256]{1,0:T(8,128)(2,1)}) custom-call(bf16[128,2048]{1,0:T(8,128)(2,1)} %x_ref.1, bf16[128,2048]{1,0:T(8,128)(2,1)} %c_ref.1, bf16[256,2048]{1,0:T(8,128)(2,1)} %u_ref.1, bf16[2048,256]{1,0:T(8,128)(2,1)} %d_ref.1), custom_call_target="tpu_custom_call" | custom-call | tf_op jit(solution)/shard_map/pallas_call | solution.py:932
  157.0 0.0 copy-start
  157.0 2.9 %convert_multiply_fusion.1 = f32[256,2048]{1,0:T(8,128)} fusion(bf16[256,2048]{1,0:T(8,128)(2,1)} %get-tuple-element.7), kind=kLoop, calls=%fused_computation.1 | loop fusion | flops 1048576 | bytes 3145728 | tf_op jit(solution)/shard_map/mul | solution.py:948
  159.8 0.0 copy-done
  159.8 0.0 copy-start.1
  159.8 1.5 convert_multiply_fusion
  161.3 0.0 copy-done.1
  161.3 0.8 copy.8
Async XLA Ops:
  157.0 2.9 %copy-start = (bf16[2048,256]{1,0:T(8,128)(2,1)S(1)}, bf16[2048,256]{1,0:T(8,128)(2,1)}, u32[]{:S(2)}) copy-start(bf16[2048,256]{1,0:T(8,128)(2,1)} %get-tuple-element.8) | copy-start | bytes 3145732
  159.8 1.5 copy-start.1

commit v2 on v1

--- a/solution.py
+++ b/solution.py
@@ -355,9 +355,9 @@
     x_ref, c_ref, u_ref, d_ref,
     ig_ref, gu_ref, gd_ref,
     xg, cg, xt, ug, dg, pre, pg, at,
-    igp, itr, isum, ira, irb, ipt, ift, su, sd, ru, rd, fu, fd,
+    igp, itr, isum0, isum1, ira, irb, ipt0, ipt1, ift0, ift1, igo, su, sd, ru, rd, fu, fd, uo, do, yu, yd,
     yw_s, yw_r, zg_s, zg_r, tx_s, tx_r, ty_s, ty_r, tt_s, tt_r,
-    rs_s, rs_r, fy_s, fy_r, fx_s, fx_r, ig_s, ig_r,
+    rs_s, rs_r, fy_s, fy_r, fx_s, fx_r, ig_s, ig_r, ld_s, st_s,
 ):
     r, f, t = lax.axis_index("rep"), lax.axis_index("fs"), lax.axis_index("tp")
     z, y = lax.div(f, 2), lax.rem(f, 2)
@@ -376,18 +376,7 @@
     near = (jnp.where(low, 0, 1), jnp.where(low, 1, -1))
     far = (1 - near[0], -near[1])
 
-    barrier = pltpu.get_barrier_semaphore()
-
-    def greet(dev):
-        pl.semaphore_signal(barrier, inc=1, device_id=dev, device_id_type=MESH)
-
-    for dev in (xdev, ydev, tdev):
-        greet(dev)
     ahead = {1: z < Z - 1, -1: z > 0}
-    for s in (1, -1):
-        pl.when(ahead[s])(functools.partial(greet, zdev(s)))
-    pl.semaphore_wait(barrier, 3 + sum(jnp.where(ahead[s], 1, 0) for s in (1, -1)))
-
     sends = []
 
     def remote(src, dst, ssem, rsem, dev):
@@ -411,23 +400,52 @@
 
     mine, other = 2 * r + y, 2 * r + 1 - y
 
-    def own(g, q, ch):
-        return u_ref.at[:, hid(q, ch)] if g == 0 else d_ref.at[hid(q, ch), :]
-
     def held(g, ch, b):
         return ug.at[ch, blk(b), :] if g == 0 else dg.at[ch, :, blk(b)]
 
+    spare = (uo, do)
+    weights = (u_ref, d_ref)
+
+    def strip(g, ref, q, ch):
+        return ref.at[:, hid(q, ch)] if g == 0 else ref.at[hid(q, ch), :]
+
+    own_x, own_c = xg.at[pl.ds(0, tok), :], cg.at[pl.ds(0, tok), :]
+    loads = {}
+    for ch in range(C):
+        for g in range(2):
+            loads["other", ch, g] = (strip(g, weights[g], other, ch), spare[g].at[ch])
+            loads["mine", ch, g] = (strip(g, weights[g], mine, ch), held(g, ch, f))
+        if ch == 0:
+            loads["x"] = (x_ref, own_x)
+            loads["c"] = (c_ref, own_c)
+    loads = {
+        key: pltpu.make_async_copy(src, dst, ld_s.at[i])
+        for i, (key, (src, dst)) in enumerate(loads.items())
+    }
+    for copy in loads.values():
+        copy.start()
+
+    barrier = pltpu.get_barrier_semaphore()
+
+    def greet(dev):
+        pl.semaphore_signal(barrier, inc=1, device_id=dev, device_id_type=MESH)
+
+    for dev in (xdev, ydev, tdev):
+        greet(dev)
+    for s in (1, -1):
+        pl.when(ahead[s])(functools.partial(greet, zdev(s)))
+    pl.semaphore_wait(barrier, 3 + sum(jnp.where(ahead[s], 1, 0) for s in (1, -1)))
+
     def swap(ch, g):
-        return remote(own(g, other, ch), held(g, ch, f), yw_s.at[ch, g], yw_r.at[ch, g], ydev)
+        return remote(spare[g].at[ch], held(g, ch, f), yw_s.at[ch, g], yw_r.at[ch, g], ydev)
 
     def origin(s, k, e):
         return f - 2 * s * k + e * (1 - 2 * y)
 
     def pass_on(ch, g, s, k, e):
         block = held(g, ch, origin(s, k, e))
-        src = own(g, mine, ch) if k == 0 and e == 0 else block
         i = (ch, (1 - s) // 2, k, e, g)
-        return remote(src, block, zg_s.at[i], zg_r.at[i], zdev(s))
+        return remote(block, block, zg_s.at[i], zg_r.at[i], zdev(s))
 
     def landed(ch, g, s, k, e):
         block = held(g, ch, origin(s, k, e))
@@ -446,10 +464,16 @@
         reached[1, k], reached[-1, k] = z >= k, z < Z - k
     passing = {key: reached[key] & ahead[key[0]] for key in reached}
 
-    def relay(ch, g, k):
-        for e in range(2):
+    outward = {1: low, -1: jnp.logical_not(low)}
+    split = {}
+    for (s, k), cond in passing.items():
+        split[s, k, 0] = cond & outward[s]
+        split[s, k, 1] = cond & outward[-s]
+
+    def relay(ch, g, k, es=(0, 1), toward=None):
+        for e in es:
             for s in (1, -1):
-                cond = passing[s, k]
+                cond = passing[s, k] if toward is None else split[s, k, toward]
 
                 @pl.when(cond)
                 def _():
@@ -477,15 +501,12 @@
 
     A, B, AB = (0, 1), (1, 2), (0, 2)
 
-    def hop(sems, i, dev, full, src, dst, cols, ref=None):
+    def hop(sems, i, dev, full, src, dst, cols):
         def make():
             where = slice(None) if cols is None else quarter(cols)
-            if ref is None:
-                take = full.at[rows(*src), where]
-            else:
-                take = ref.at[pl.ds(src[2][0] * half, (src[2][1] - src[2][0]) * half), where]
             return remote(
-                take, full.at[rows(*dst), where], sems[0].at[i], sems[1].at[i], dev
+                full.at[rows(*src), where], full.at[rows(*dst), where],
+                sems[0].at[i], sems[1].at[i], dev,
             )
 
         return make
@@ -493,16 +514,16 @@
     X, Y, S = (tx_s, tx_r), (ty_s, ty_r), (tt_s, tt_r)
     moves = {}
     for i, part in enumerate((A, B)):
-        moves["x", "x", i] = hop(X, i, xdev, xg, (0, 0, part), (1, 0, part), None, x_ref)
-        moves["y", "x", i] = hop(Y, i, ydev, xg, (0, 0, part), (2, 0, part), None, x_ref)
+        moves["x", "x", i] = hop(X, i, xdev, xg, (0, 0, part), (1, 0, part), None)
+        moves["y", "x", i] = hop(Y, i, ydev, xg, (0, 0, part), (2, 0, part), None)
         moves["d", "x", i] = hop(X, 2 + i, xdev, xg, (2, 0, part), (3, 0, part), None)
-    moves["s", "x", 0] = hop(S, 0, tdev, xg, (0, 0, AB), (0, 1, AB), None, x_ref)
-    moves["s", "c", 0] = hop(S, 1, tdev, cg, (0, 0, AB), (0, 1, AB), None, c_ref)
+    moves["s", "x", 0] = hop(S, 0, tdev, xg, (0, 0, AB), (0, 1, AB), None)
+    moves["s", "c", 0] = hop(S, 1, tdev, cg, (0, 0, AB), (0, 1, AB), None)
     for k in range(1, 4):
         moves["s", "x", k] = hop(S, 1 + k, tdev, xg, (k, 0, AB), (k, 1, AB), None)
     for i in range(Z):
-        moves["x", "c", i] = hop(X, 4 + 2 * i, xdev, cg, (0, 0, AB), (1, 0, AB), i, c_ref)
-        moves["y", "c", i] = hop(Y, 2 + 2 * i, ydev, cg, (0, 0, AB), (2, 0, AB), i, c_ref)
+        moves["x", "c", i] = hop(X, 4 + 2 * i, xdev, cg, (0, 0, AB), (1, 0, AB), i)
+        moves["y", "c", i] = hop(Y, 2 + 2 * i, ydev, cg, (0, 0, AB), (2, 0, AB), i)
         moves["dx", "c", i] = hop(X, 5 + 2 * i, xdev, cg, (2, 0, A), (3, 0, A), i)
         moves["dy", "c", i] = hop(Y, 3 + 2 * i, ydev, cg, (1, 0, B), (3, 0, B), i)
         for k in range(1, 4):
@@ -545,160 +566,177 @@
 
     out_buf, in_buf, fin = (su, sd), (ru, rd), (fu, fd)
 
-    def partial_copy(ch, g, way, j):
+    def partial_copy(ch, g, way, j, e):
         d, s = way
         return remote(
-            out_buf[g].at[d, j, ch], in_buf[g].at[d, j, ch],
-            rs_s.at[d, j, ch, g], rs_r.at[d, j, ch, g], zdev(s))
+            out_buf[g].at[d, j, ch, e], in_buf[g].at[d, j, ch, e],
+            rs_s.at[d, j, ch, g, e], rs_r.at[d, j, ch, g, e], zdev(s))
+
+    def side_of(e):
+        return e * y + (1 - e) * (1 - y)
 
     def reduce(ch, g, way, j, m0):
         cond = level[m0]
         to = jnp.where(way[1] > 0, Z - 1 - j, j)
-        make = functools.partial(partial_copy, ch, g, way, j)
         more = m0 > 0 or way is far
-        if more:
-            make().wait_recv()
 
         @pl.loop(0, 2)
-        def _(h):
-            val = grad(ch, g, 2 * to + h)
+        def _(e):
+            val = grad(ch, g, 2 * to + side_of(e))
             if more:
-                val = val + in_buf[g][way[0], j, ch, h].astype(F32)
-            out_buf[g][way[0], j, ch, h] = val.astype(BF16)
-
-        go(make, cond)
-
-    def place(g, q, ch):
-        return gu_ref.at[:, hid(q, ch)] if g == 0 else gd_ref.at[hid(q, ch), :]
+                partial_copy(ch, g, way, j, e).wait_recv()
+                val = val + in_buf[g][way[0], j, ch, e].astype(F32)
+            out_buf[g][way[0], j, ch, e] = val.astype(BF16)
+            partial_copy(ch, g, way, j, e).start()
+
+        for e in range(2):
+            sends.append((cond, functools.partial(partial_copy, ch, g, way, j, e)))
+
+    outs, passed = (gu_ref, gd_ref), (yu, yd)
+
+    def store(ch, g, e):
+        if ch == C:
+            return pltpu.make_async_copy(igo, ig_ref, st_s.at[4 * C])
+        src = passed[g].at[ch] if e else fin[g].at[ch, 1]
+        dst = strip(g, outs[g], other if e else mine, ch)
+        return pltpu.make_async_copy(src, dst, st_s.at[4 * ch + 2 * g + e])
 
     def final_y(ch, g):
         return remote(
-            fin[g].at[ch, 1 - y], place(g, mine, ch), fy_s.at[ch, g], fy_r.at[ch, g], ydev)
-
-    def final_y_in(ch, g):
+            fin[g].at[ch, 0], passed[g].at[ch], fy_s.at[ch, g], fy_r.at[ch, g], ydev)
+
+    def final_x(ch, g, e):
+        src = passed[g].at[ch] if e else fin[g].at[ch, 1]
+        i = (ch, g, e)
         return remote(
-            place(g, other, ch), place(g, other, ch), fy_s.at[ch, g], fy_r.at[ch, g], ydev)
-
-    def final_x(ch, g, e):
-        src = fin[g].at[ch, y] if e == 0 else place(g, other, ch)
-        q = other if e else mine
-        i = (ch, g, e)
-        return remote(src, place(g, q, ch), fx_s.at[i], fx_r.at[i], xdev)
+            src, strip(g, outs[g], other if e else mine, ch), fx_s.at[i], fx_r.at[i], xdev)
 
     def final_x_in(ch, g, e):
         q = 2 * (1 - r) + (1 - y if e else y)
+        src = passed[g].at[ch] if e else fin[g].at[ch, 1]
         i = (ch, g, e)
-        return remote(place(g, q, ch), place(g, q, ch), fx_s.at[i], fx_r.at[i], xdev)
-
-    def finish(ch, g, m0):
+        return remote(src, strip(g, outs[g], q, ch), fx_s.at[i], fx_r.at[i], xdev)
+
+    def finish(ch, g, m0, between=None):
         cond = level[m0]
         ways = [(far, m0)] + ([(near, Z - 1 - m0)] if m0 else [])
-        for way, j in ways:
-            partial_copy(ch, g, way, j).wait_recv()
-
-        @pl.loop(0, 2)
-        def _(h):
-            val = grad(ch, g, 2 * z + h)
+        for e in range(2):
+            val = grad(ch, g, 2 * z + side_of(e))
             for way, j in ways:
-                val = val + in_buf[g][way[0], j, ch, h].astype(F32)
-            fin[g][ch, h] = val.astype(BF16)
-
-        go(functools.partial(final_y, ch, g), cond)
-        go(functools.partial(final_x, ch, g, 0), cond)
-        if g == 0:
-            gu_ref[:, hid(mine, ch)] = fu[ch, y]
-        else:
-            gd_ref[hid(mine, ch), :] = fd[ch, y]
+                partial_copy(ch, g, way, j, e).wait_recv()
+                val = val + in_buf[g][way[0], j, ch, e].astype(F32)
+            fin[g][ch, e] = val.astype(BF16)
+            if e == 0:
+                go(functools.partial(final_y, ch, g), cond)
+                if between:
+                    between()
+            else:
+                go(functools.partial(final_x, ch, g, 0), cond)
+        store(ch, g, 0).start()
 
     def spread(ch, g, m0):
-        final_y_in(ch, g).wait_recv()
+        final_y(ch, g).wait_recv()
         go(functools.partial(final_x, ch, g, 1), level[m0])
-
-    hd = D // 2
+        store(ch, g, 1).start()
+
+    h0 = isum0.shape[2]
+    cuts = ((0, h0), (h0, D))
+    isum, igot, ipt, ift = (isum0, isum1), (ira, irb), (ipt0, ipt1), (ift0, ift1)
 
     def ig_copy(i):
         if i == 0:
-            return remote(igp.at[:, pl.ds(tok, tok), :], itr, ig_s.at[0], ig_r.at[0], tdev)
+            return remote(igp.at[1], itr, ig_s.at[0], ig_r.at[0], tdev)
+        if i > 6:
+            side, part = (i - 7) % 2, pl.ds((i - 7) // 2 * half, half)
+            src, dst = isum[side].at[1 + side, part, :], igot[side].at[0, part, :]
+            return remote(src, dst, ig_s.at[i], ig_r.at[i], (xdev, ydev)[side])
         side, step = (i - 1) % 2, (i - 1) // 2
-        if step < 2:
-            src = isum.at[side, 3 if step else 1 + side]
-            dst = (ira, irb)[side].at[step]
+        if step == 1:
+            src, dst = isum[side].at[3], igot[side].at[1]
         else:
-            src, dst = ipt.at[side], ift.at[side]
+            src, dst = ipt[side], ift[side]
         dev = (xdev, ydev)[side if step < 2 else 1 - side]
         return remote(src, dst, ig_s.at[i], ig_r.at[i], dev)
 
     def ig_go(i, cond):
         go(functools.partial(ig_copy, i), cond)
 
-    def ig_partial(cond):
-        @pl.loop(0, 4)
-        def _(k):
-            part = span(k * wide, wide)
-
-            @pl.loop(0, n)
+    def ig_part(cond):
+        for dt in (1, 0):
+
+            @pl.loop(0, n, unroll=2)
             def _(b):
                 val = 0.0
                 for ch in range(C):
+                    lhs = jnp.concatenate([pg[ch, rows(k, dt), :] for k in range(4)], 0)
                     val = val + lax.dot_general(
-                        pg[ch, part, :], ug[ch, blk(b), :], NT, preferred_element_type=F32)
-                igp[k, :, blk(b)] = val.astype(BF16)
-
-        ig_go(0, cond)
+                        lhs, ug[ch, blk(b), :], NT, preferred_element_type=F32)
+                val = val.astype(BF16)
+                for k in range(4):
+                    igp[dt, k, :, blk(b)] = val[k * tok:(k + 1) * tok]
+
+            if dt:
+                ig_go(0, cond)
 
     def ig_first(cond):
         ig_copy(0).wait_recv()
 
         @pl.loop(0, 4)
         def _(k):
-            for side in range(2):
-                cols = pl.ds(side * hd, hd)
-                val = igp[k, 0:tok, cols].astype(F32) + itr[k, :, cols].astype(F32)
-                isum[side, k] = val.astype(BF16)
-
-        for i in range(1, 5):
+            val = igp[0, k].astype(F32) + itr[k].astype(F32)
+            for side, (lo, hi) in enumerate(cuts):
+                isum[side][k] = val[:, lo:hi].astype(BF16)
+
+        for i in (4, 3):
             ig_go(i, cond)
 
+    def ig_more(cond, part):
+        for side in range(2):
+            ig_go(7 + 2 * part + side, cond)
+
     def ig_second(cond):
-        for i in range(1, 5):
-            ig_copy(i).wait_recv()
-        for side, got in enumerate((ira, irb)):
-            val = isum[side, 2 - side].astype(F32) + got[1].astype(F32)
-            ipt[side] = val.astype(BF16)
+        for side in range(2):
+            ig_copy(3 + side).wait_recv()
+            val = isum[side][2 - side].astype(F32) + igot[side][1].astype(F32)
+            ipt[side][...] = val.astype(BF16)
             ig_go(5 + side, cond)
 
     def ig_last():
-        for side, got in enumerate((ira, irb)):
-            ig_copy(5 + side).wait_recv()
-            val = isum[side, 0].astype(F32) + got[0].astype(F32) + ift[side].astype(F32)
-            ig_ref[:, side * hd:(side + 1) * hd] = val.astype(BF16)
+        for side, (lo, hi) in enumerate(cuts):
+            for i in (5, 7, 9):
+                ig_copy(i + side).wait_recv()
+            val = isum[side][0].astype(F32) + igot[side][0].astype(F32)
+            igo[:, lo:hi] = (val + ift[side][...].astype(F32)).astype(BF16)
+        store(C, 0, 0).start()
 
     edge, inner = level[0], m > 0
     last = C - 1
 
+    units = [(ch, g) for ch in range(C) for g in range(2)]
+
+    loads["other", 0, 0].wait()
+    go(functools.partial(swap, 0, 0))
+    loads["mine", 0, 0].wait()
     begin(0, 0, 0)
-    go(functools.partial(swap, 0, 0))
+    loads["x"].wait()
     for i in range(2):
         start("x", "x", i)
         start("y", "x", i)
+    loads["mine", 0, 1].wait()
     begin(0, 1, 0, edge)
     start("s", "x", 0)
+    loads["c"].wait()
     start("s", "c", 0)
-    for ch in range(C):
-        for g in range(2):
-            if ch or g:
-                go(functools.partial(swap, ch, g))
-    xg[0:tok, :] = x_ref[...]
-    cg[0:tok, :] = c_ref[...]
-    for ch in range(C):
-        ug[ch, blk(f), :] = u_ref[:, hid(mine, ch)]
-        dg[ch, :, blk(f)] = d_ref[hid(mine, ch), :]
+    for unit in units[1:]:
+        loads[("other",) + unit].wait()
+        go(functools.partial(swap, *unit))
+        if unit != units[1]:
+            loads[("mine",) + unit].wait()
 
     swap(0, 0).wait_recv()
     begin(0, 0, 1)
-    for ch in range(1, C):
-        for g in range(2):
-            begin(ch, g, 0, edge)
+    for unit in units[2:]:
+        begin(*unit, 0, edge)
     relay(0, 0, 1)
     arrive("s", "x", 0)
     arrive("s", "c", 0)
@@ -707,68 +745,101 @@
     start("d", "x", 0)
     for k in range(2, Z - 1):
         relay(0, 0, k)
-    begin(0, 1, 0, inner)
+    for unit in units[1:3]:
+        begin(*unit, 0, inner)
     for i in range(2):
         arrive("x", "x", i)
     start("s", "x", 1)
     arrive("y", "x", 1)
     start("d", "x", 1)
-    start("x", "c", 0)
-    start("y", "c", 0)
+    for i in range(min(2, Z)):
+        start("x", "c", i)
+        start("y", "c", i)
     start("s", "x", 2)
     swap(0, 1).wait_recv()
     begin(0, 1, 1)
+    relay(0, 1, 1, (0,))
     arrive("s", "x", 1)
     flip(1)
+    for k in range(2, Z - 1):
+        relay(0, 1, k, (0,))
+    relay(0, 1, 1, (1,))
     arrive("s", "x", 2)
     flip(2)
-    relay(0, 1, 1)
     collect(0, 0)
     forward(0, 0, 3)
-    for ch in range(1, C):
-        for g in range(2):
-            swap(ch, g).wait_recv()
-            begin(ch, g, 1, edge)
+    for unit in units[2:]:
+        swap(*unit).wait_recv()
+        begin(*unit, 1, edge)
     for i in range(2):
         arrive("d", "x", i)
     start("s", "x", 3)
-    for k in range(2, Z - 1):
-        relay(0, 1, k)
-    for ch in range(1, C):
-        begin(ch, 0, 0, inner)
-        begin(ch, 0, 1, inner)
-    arrive("s", "x", 3)
-    flip(3)
-    forward(0, 3, 4)
+
+    def ready(i):
+        for k in range(1, 4):
+            arrive("s%d" % k, "c", i)
+        if i < Z - 1:
+            pl.when(edge)(functools.partial(reduce, 0, 1, near, i, 0))
+
+    tasks = [(unit, k) for unit in units[2:] for k in range(1, Z - 1)]
     for i in range(Z):
-        if i + 1 < Z:
-            start("x", "c", i + 1)
-            start("y", "c", i + 1)
         arrive("x", "c", i)
         start("dy", "c", i)
         start("s1", "c", i)
         arrive("y", "c", i)
         start("dx", "c", i)
         start("s2", "c", i)
-        if 1 <= i < Z - 1:
-            for ch in range(1, C):
-                relay(ch, 0, i)
-                if i == Z - 2:
-                    begin(ch, 1, 0, inner)
-                    begin(ch, 1, 1, inner)
+        if i + 2 < Z:
+            start("x", "c", i + 2)
+            start("y", "c", i + 2)
+        if i == 0:
+            for k in range(2, Z - 1):
+                relay(0, 1, k, (1,))
+            for unit in units[2:]:
+                if unit != units[2]:
+                    begin(*unit, 0, inner)
+                begin(*unit, 1, inner)
+            for unit in units[2:]:
+                for k in range(1, Z // 2):
+                    relay(*unit, k, toward=0)
+            arrive("s", "x", 3)
+            flip(3)
+            forward(0, 3, 4)
+        else:
+            ready(i - 1)
+            if i == Z - 1:
+                for m0 in range(1, Z // 2):
+                    pl.when(level[m0])(functools.partial(reduce, 0, 1, near, 0, m0))
         arrive("dy", "c", i)
         arrive("dx", "c", i)
         start("s3", "c", i)
-        for k in range(1, 4):
-            arrive("s%d" % k, "c", i)
-        if i < Z - 1:
-            pl.when(edge)(functools.partial(reduce, 0, 1, near, i, 0))
-    collect(0, 1)
-    backward(0)
+        if i == 1 and tasks:
+            unit, k = tasks.pop(0)
+            relay(*unit, k, toward=1)
+    ready(Z - 1)
+
+    early = list(sends)
+    sends.clear()
+
+    def drain(some):
+        for cond, make in some:
+            if cond is None:
+                make().wait_send()
+            else:
+                pl.when(cond)(lambda: make().wait_send())
+
+    def flush(base, count):
+        some = sends[base:count]
+        del sends[base:count]
+        drain(some)
 
     def edges():
+        base = len(sends)
+        collect(0, 1)
+        backward(0)
         for j in range(Z - 1):
             reduce(0, 0, near, j, 0)
+        drain(early)
         for ch in range(1, C):
             collect(ch, 0)
             forward(ch, 0, 4)
@@ -776,87 +847,116 @@
                 reduce(ch, 1, near, j, 0)
             collect(ch, 1)
             backward(ch)
-            for j in range(Z - 1):
-                reduce(ch, 0, near, j, 0)
-        ig_partial(edge)
+            if ch < C - 1:
+                for j in range(Z - 1):
+                    reduce(ch, 0, near, j, 0)
+        count = len(sends)
+        ig_part(edge)
         finish(0, 1, 0)
         ig_first(edge)
+        if C > 1:
+            for j in range(Z - 1):
+                reduce(C - 1, 0, near, j, 0)
+        finish(0, 0, 0)
         spread(0, 1, 0)
-        finish(0, 0, 0)
-        ig_second(edge)
-        spread(0, 0, 0)
         for ch in range(1, C):
             finish(ch, 1, 0)
             if ch == 1:
-                ig_last()
-            spread(ch, 1, 0)
-            finish(ch, 0, 0)
-            spread(ch, 0, 0)
+                ig_second(edge)
+            spread(ch - 1, 0, 0)
+            if ch == 1:
+                ig_more(edge, 0)
+                flush(base, count)
+            finish(ch, 0, 0, lambda: spread(ch, 1, 0))
+            if ch == 1:
+                ig_more(edge, 1)
+        if C == 1:
+            ig_second(edge)
+            ig_more(edge, 0)
+            ig_more(edge, 1)
+        spread(C - 1, 0, 0)
+        ig_last()
 
     def inside(m0):
-        cond = level[m0]
-
-        def some(ch, g):
-            for j in range(Z - 1 - m0):
+        cond, base = level[m0], len(sends)
+        left = list(tasks)
+
+        def relays(count):
+            for _ in range(min(count, len(left))):
+                unit, k = left.pop(0)
+                relay(*unit, k, toward=1)
+
+        def nears(ch, g, js):
+            for j in js:
                 reduce(ch, g, near, j, m0)
-                if j < m0:
-                    reduce(ch, g, far, j, m0)
-
-        for j in range(Z - 1 - m0):
-            reduce(0, 1, near, j, m0)
-            if j + 1 < Z - 1:
-                for ch in range(1, C):
-                    relay(ch, 1, j + 1)
-        for ch in range(1, C):
-            for k in range(Z - m0, Z - 1):
-                relay(ch, 1, k)
-        for j in range(m0):
-            reduce(0, 1, far, j, m0)
+
+        def fars(ch, g):
+            for j in range(m0):
+                reduce(ch, g, far, j, m0)
+
+        first, rest = range(1), range(1, Z - 1 - m0)
+        keep = (Z - 2) * (C > 1)
+        relays(len(left) - keep)
+        nears(0, 1, rest)
+        relays(keep - 1)
+        backward(0)
         for ch in range(1, C):
             forward(ch, 0, 4)
+        relays(1)
+        fars(0, 1)
+        for ch in range(1, C):
             backward(ch)
-        ig_partial(cond)
-        reduce(0, 0, near, 0, m0)
-        ig_first(cond)
+        nears(0, 0, first)
         finish(0, 1, m0)
-        for j in range(1, Z - 1 - m0):
-            reduce(0, 0, near, j, m0)
+        nears(0, 0, rest)
         spread(0, 1, m0)
-        for j in range(m0):
-            reduce(0, 0, far, j, m0)
-        ig_second(cond)
+        fars(0, 0)
+        ig_part(cond)
+        drain(early)
         finish(0, 0, m0)
         for ch in range(1, C):
-            reduce(ch, 1, near, 0, m0)
+            nears(ch, 1, first)
             if ch == 1:
-                spread(0, 0, m0)
-                ig_last()
-            for j in range(1, Z - 1 - m0):
-                reduce(ch, 1, near, j, m0)
-            for j in range(m0):
-                reduce(ch, 1, far, j, m0)
+                ig_first(cond)
+            spread(ch - 1, 0, m0)
+            if ch == 1:
+                ig_more(cond, 0)
+            nears(ch, 1, rest)
+            fars(ch, 1)
+            if ch == 1:
+                ig_second(cond)
             finish(ch, 1, m0)
-            reduce(ch, 0, near, 0, m0)
+            count = len(sends)
+            nears(ch, 0, (0, *rest))
+            fars(ch, 0)
+            if ch == 1:
+                ig_more(cond, 1)
             spread(ch, 1, m0)
-            for j in range(1, Z - 1 - m0):
-                reduce(ch, 0, near, j, m0)
-            for j in range(m0):
-                reduce(ch, 0, far, j, m0)
+            if ch == C - 1:
+                flush(base, count)
             finish(ch, 0, m0)
-            spread(ch, 0, m0)
+        if C == 1:
+            ig_first(cond)
+            ig_more(cond, 0)
+            ig_more(cond, 1)
+            ig_second(cond)
+        spread(C - 1, 0, m0)
+        ig_last()
 
     pl.when(edge)(edges)
     for m0 in range(1, Z // 2):
         pl.when(level[m0])(functools.partial(inside, m0))
-    for ch in range(C):
-        for g in (1, 0):
-            for e in range(2):
-                final_x_in(ch, g, e).wait_recv()
-    for cond, make in sends:
-        if cond is None:
-            make().wait_send()
-        else:
-            pl.when(cond)(lambda: make().wait_send())
+
+    def settle():
+        for ch in range(C):
+            for g in (1, 0):
+                for e in range(2):
+                    final_x_in(ch, g, e).wait_recv()
+                    store(ch, g, e).wait()
+        store(C, 0, 0).wait()
+
+    settle()
+    drain(sends)
 
 
 def ring_call(inputs, up_weight):
@@ -883,7 +983,7 @@
         S((2, R)), S((2, R)), S((2, T, R)), S((2, T, R)),
         S((T,)), S((T,)), S((R,)), S((R,)), S((C, 2, R)), S((C, 2, R)),
     ]
-    return functools.partial(ring_kernel, R, n, T), scratch, (R, hb)
+    return functools.partial(ring_kernel, R, n, T), scratch, (R, hb), pltpu.VMEM
 
 
 def axis_sizes():
@@ -895,40 +995,46 @@
     tok, D = inputs.shape
     db, HB = up_weight.shape
     Z, G = n // 2, 2 * R
-    if R != 2 or T != 2 or n % 4 or tok % 32 or HB % (128 * G) or db % 128:
+    if R != 2 or T != 2 or n % 4 or tok % 32 or HB % (128 * G) or db % 128 or D % 1024:
         return None
     hw = HB // G
     C = tile_of(hw // 128, CHUNKS)
     hc = hw // C
-    rows, hd = 8 * tok, D // 2
+    rows, h0 = 8 * tok, D // 8
+    h1 = D - h0
     V, S = pltpu.VMEM, pltpu.SemaphoreType.DMA
     data = [
         ((rows, D), BF16), ((rows, D), BF16), ((D, rows), BF16),
         ((C, D, hc), BF16), ((C, hc, D), BF16),
         ((C, rows, hc), F32), ((C, rows, hc), BF16), ((C, hc, rows), BF16),
-        ((4, 2 * tok, D), BF16), ((4, tok, D), BF16), ((2, 4, tok, hd), BF16),
-        ((2, tok, hd), BF16), ((2, tok, hd), BF16), ((2, tok, hd), BF16), ((2, tok, hd), BF16),
+        ((2, 4, tok, D), BF16), ((4, tok, D), BF16), ((4, tok, h0), BF16), ((4, tok, h1), BF16),
+        ((2, tok, h0), BF16), ((2, tok, h1), BF16), ((tok, h0), BF16), ((tok, h1), BF16),
+        ((tok, h0), BF16), ((tok, h1), BF16),
+        ((tok, D), BF16),
         ((2, Z - 1, C, 2, db, hc), BF16), ((2, Z - 1, C, 2, hc, db), BF16),
         ((2, Z - 1, C, 2, db, hc), BF16), ((2, Z - 1, C, 2, hc, db), BF16),
         ((C, 2, db, hc), BF16), ((C, 2, hc, db), BF16),
+        ((C, db, hc), BF16), ((C, hc, db), BF16), ((C, db, hc), BF16), ((C, hc, db), BF16),
     ]
     size = sum(math.prod(s) * jnp.dtype(d).itemsize for s, d in data)
     if size > 50 * 2**20:
         return None
     sems = [
         (C, 2), (C, 2, Z - 1, 2, 2), (4 + 2 * Z,), (2 + 2 * Z,), (5 + 3 * Z,),
-        (2, Z - 1, C, 2), (C, 2), (C, 2, 2), (7,),
+        (2, Z - 1, C, 2, 2), (C, 2), (C, 2, 2), (11,),
     ]
     scratch = [V(s, d) for s, d in data] + [S(s) for s in sems for _ in range(2)]
-    return functools.partial(plane_kernel, Z), scratch, (1, HB)
+    scratch += [S((4 * C + 2,)), S((4 * C + 1,))]
+    return functools.partial(plane_kernel, Z), scratch, (1, HB), pl.ANY
 
 
 def shards(inputs, cotangent, up_weight, down_weight):
     R, n, T = axis_sizes()
     tok, D = inputs.shape
     db = up_weight.shape[0]
-    body, scratch, (parts, hb) = plane_call(inputs, up_weight) or ring_call(inputs, up_weight)
-    vmem = pl.BlockSpec(memory_space=pltpu.VMEM)
+    chosen = plane_call(inputs, up_weight) or ring_call(inputs, up_weight)
+    body, scratch, (parts, hb), space = chosen
+    spec = pl.BlockSpec(memory_space=space)
     ig, gu, gd = pl.pallas_call(
         body,
         out_shape=(
@@ -936,8 +1042,8 @@
             jax.ShapeDtypeStruct((db, parts * hb), BF16),
             jax.ShapeDtypeStruct((parts * hb, db), BF16),
         ),
-        in_specs=[vmem] * 4,
-        out_specs=(vmem,) * 3,
+        in_specs=[spec] * 4,
+        out_specs=(spec,) * 3,
         scratch_shapes=scratch,
         compiler_params=pltpu.CompilerParams(
             collective_id=0, has_side_effects=True, vmem_limit_bytes=60 * 2**20

time: 162 us -> 131 us (0.81)
  Pallas kernels: 156 us -> 125 us
    pallas_call x1, Pallas kernels: 156 us -> 125 us  [shards(): pl.pallas_call(body, out_shape=(jax.ShapeDtypeStruct((tok, D), BF16), jax...]
where the time goes in v2:
time: 131 us
  Pallas kernels  125 us (95%)
  other arithmetic  4.33 us (3%)
    pallas_call x1, Pallas kernels, shards(): pl.pallas_call(body, out_shape=(jax.ShapeDtypeStruct((tok, D), BF16), jax...  125 us
    mul x2, other arithmetic, shards(): return (ig, gu.astype(F32) * loss_scale, gd.astype(F32) * loss_scale)  4.33 us

profile of v2, /device:TPU:0, one launch (start us, length us, event | category | flops | bytes accessed | tf_op | source)
XLA Modules:
  0.0 130.9 jit_solution(2827153110925783089)
XLA Ops:
  0.6 125.2 %shard_map.67 = (bf16[128,2048]{1,0:T(8,128)(2,1)}, bf16[256,2048]{1,0:T(8,128)(2,1)}, bf16[2048,256]{1,0:T(8,128)(2,1)}) custom-call(bf16[128,2048]{1,0:T(8,128)(2,1)} %x_ref.1, bf16[128,2048]{1,0:T(8,128)(2,1)} %c_ref.1, bf16[256,2048]{1,0:T(8,128)(2,1)} %u_ref.1, bf16[2048,256]{1,0:T(8,128)(2,1)} %d_ref.1), custom_call_target="tpu_custom_call" | custom-call | tf_op jit(solution)/shard_map/pallas_call | solution.py:1038
  125.8 0.0 copy-start
  125.8 2.9 %convert_multiply_fusion.1 = f32[256,2048]{1,0:T(8,128)} fusion(bf16[256,2048]{1,0:T(8,128)(2,1)} %get-tuple-element.7), kind=kLoop, calls=%fused_computation.1 | loop fusion | flops 1048576 | bytes 3145728 | tf_op jit(solution)/shard_map/mul | solution.py:1054
  128.7 0.0 copy-done
  128.7 0.0 copy-start.1
  128.7 1.5 %convert_multiply_fusion = f32[2048,256]{1,0:T(8,128)} fusion(bf16[2048,256]{1,0:T(8,128)(2,1)S(1)} %copy-done), kind=kLoop, calls=%fused_computation | loop fusion | flops 1048576 | bytes 3145728 | tf_op jit(solution)/shard_map/mul | solution.py:1054
  130.2 0.0 copy-done.1
  130.2 0.8 copy.8
Async XLA Ops:
  125.8 2.9 %copy-start = (bf16[2048,256]{1,0:T(8,128)(2,1)S(1)}, bf16[2048,256]{1,0:T(8,128)(2,1)}, u32[]{:S(2)}) copy-start(bf16[2048,256]{1,0:T(8,128)(2,1)} %get-tuple-element.8) | copy-start | bytes 3145732
  128.7 1.5 %copy-start.1 = (bf16[128,2048]{1,0:T(8,128)(2,1)S(1)}, bf16[128,2048]{1,0:T(8,128)(2,1)}, u32[]{:S(2)}) copy-start(bf16[128,2048]{1,0:T(8,128)(2,1)} %get-tuple-element.12) | copy-start | bytes 1572868

commit v3 on v2

--- a/solution.py
+++ b/solution.py
@@ -355,9 +355,8 @@
     x_ref, c_ref, u_ref, d_ref,
     ig_ref, gu_ref, gd_ref,
     xg, cg, xt, ug, dg, pre, pg, at,
-    igp, itr, isum0, isum1, ira, irb, ipt0, ipt1, ift0, ift1, igo, su, sd, ru, rd, fu, fd, uo, do, yu, yd,
-    yw_s, yw_r, zg_s, zg_r, tx_s, tx_r, ty_s, ty_r, tt_s, tt_r,
-    rs_s, rs_r, fy_s, fy_r, fx_s, fx_r, ig_s, ig_r, ld_s, st_s,
+    igp, itr, isum, igot, ipt, ift, igo, su, sd, ru, rd, fu, fd, uo, do, yu, yd,
+    out_s, yw_r, zg_r, tx_r, ty_r, tt_r, rs_r, fy_r, fx_r, ig_r, ld_s, st_s,
 ):
     r, f, t = lax.axis_index("rep"), lax.axis_index("fs"), lax.axis_index("tp")
     z, y = lax.div(f, 2), lax.rem(f, 2)
@@ -377,7 +376,6 @@
     far = (1 - near[0], -near[1])
 
     ahead = {1: z < Z - 1, -1: z > 0}
-    sends = []
 
     def remote(src, dst, ssem, rsem, dev):
         return pltpu.make_async_remote_copy(
@@ -385,9 +383,8 @@
             device_id=dev, device_id_type=MESH,
         )
 
-    def go(make, cond=None):
+    def go(make):
         make().start()
-        sends.append((cond, make))
 
     def span(at_, size):
         return pl.ds(pl.multiple_of(at_, size), size)
@@ -437,7 +434,7 @@
     pl.semaphore_wait(barrier, 3 + sum(jnp.where(ahead[s], 1, 0) for s in (1, -1)))
 
     def swap(ch, g):
-        return remote(spare[g].at[ch], held(g, ch, f), yw_s.at[ch, g], yw_r.at[ch, g], ydev)
+        return remote(spare[g].at[ch], held(g, ch, f), out_s.at[0], yw_r.at[ch, g], ydev)
 
     def origin(s, k, e):
         return f - 2 * s * k + e * (1 - 2 * y)
@@ -445,18 +442,18 @@
     def pass_on(ch, g, s, k, e):
         block = held(g, ch, origin(s, k, e))
         i = (ch, (1 - s) // 2, k, e, g)
-        return remote(block, block, zg_s.at[i], zg_r.at[i], zdev(s))
+        return remote(block, block, out_s.at[i[1] + 1], zg_r.at[i], zdev(s))
 
     def landed(ch, g, s, k, e):
         block = held(g, ch, origin(s, k, e))
         i = (ch, (1 - s) // 2, k - 1, e, g)
-        return remote(block, block, zg_s.at[i], zg_r.at[i], zdev(s))
+        return remote(block, block, out_s.at[i[1] + 1], zg_r.at[i], zdev(s))
 
     def begin(ch, g, e, also=None):
         for s in (1, -1):
             cond = ahead[s] if also is None else ahead[s] & also
             pl.when(cond)(functools.partial(
-                go, functools.partial(pass_on, ch, g, s, 0, e), cond))
+                go, functools.partial(pass_on, ch, g, s, 0, e)))
 
     level = [m == m0 for m0 in range(Z // 2)]
     reached = {}
@@ -478,7 +475,7 @@
                 @pl.when(cond)
                 def _():
                     landed(ch, g, s, k, e).wait_recv()
-                    go(functools.partial(pass_on, ch, g, s, k, e), cond)
+                    go(functools.partial(pass_on, ch, g, s, k, e))
 
     def collect(ch, g):
         for k in range(1, Z):
@@ -506,12 +503,12 @@
             where = slice(None) if cols is None else quarter(cols)
             return remote(
                 full.at[rows(*src), where], full.at[rows(*dst), where],
-                sems[0].at[i], sems[1].at[i], dev,
+                sems[0], sems[1].at[i], dev,
             )
 
         return make
 
-    X, Y, S = (tx_s, tx_r), (ty_s, ty_r), (tt_s, tt_r)
+    X, Y, S = (out_s.at[3], tx_r), (out_s.at[4], ty_r), (out_s.at[5], tt_r)
     moves = {}
     for i, part in enumerate((A, B)):
         moves["x", "x", i] = hop(X, i, xdev, xg, (0, 0, part), (1, 0, part), None)
@@ -522,10 +519,11 @@
     for k in range(1, 4):
         moves["s", "x", k] = hop(S, 1 + k, tdev, xg, (k, 0, AB), (k, 1, AB), None)
     for i in range(Z):
-        moves["x", "c", i] = hop(X, 4 + 2 * i, xdev, cg, (0, 0, AB), (1, 0, AB), i)
-        moves["y", "c", i] = hop(Y, 2 + 2 * i, ydev, cg, (0, 0, AB), (2, 0, AB), i)
-        moves["dx", "c", i] = hop(X, 5 + 2 * i, xdev, cg, (2, 0, A), (3, 0, A), i)
-        moves["dy", "c", i] = hop(Y, 3 + 2 * i, ydev, cg, (1, 0, B), (3, 0, B), i)
+        for p, (xp, yp) in enumerate(((B, A), (A, B))):
+            moves["x%d" % p, "c", i] = hop(X, 4 + 3 * i + p, xdev, cg, (0, 0, xp), (1, 0, xp), i)
+            moves["y%d" % p, "c", i] = hop(Y, 2 + 3 * i + p, ydev, cg, (0, 0, yp), (2, 0, yp), i)
+        moves["dx", "c", i] = hop(X, 6 + 3 * i, xdev, cg, (2, 0, A), (3, 0, A), i)
+        moves["dy", "c", i] = hop(Y, 4 + 3 * i, ydev, cg, (1, 0, B), (3, 0, B), i)
         for k in range(1, 4):
             moves["s%d" % k, "c", i] = hop(
                 S, 5 + (k - 1) * Z + i, tdev, cg, (k, 0, AB), (k, 1, AB), i)
@@ -544,7 +542,7 @@
             xt[blk(b), part] = xg[part, blk(b)].T
 
     def forward(ch, first, last):
-        @pl.loop(first, last)
+        @pl.loop(first, last, unroll=2 if (last - first) % 2 == 0 else 1)
         def _(k):
             part = span(k * wide, wide)
             active = jnp.maximum(
@@ -553,7 +551,7 @@
             at[ch, :, part] = (active * active).astype(BF16).T
 
     def backward(ch):
-        @pl.loop(0, 4)
+        @pl.loop(0, 4, unroll=2)
         def _(k):
             part = span(k * wide, wide)
             val = lax.dot_general(cg[part, :], dg[ch], NT, preferred_element_type=F32)
@@ -570,7 +568,7 @@
         d, s = way
         return remote(
             out_buf[g].at[d, j, ch, e], in_buf[g].at[d, j, ch, e],
-            rs_s.at[d, j, ch, g, e], rs_r.at[d, j, ch, g, e], zdev(s))
+            out_s.at[6], rs_r.at[d, j, ch, g, e], zdev(s))
 
     def side_of(e):
         return e * y + (1 - e) * (1 - y)
@@ -589,9 +587,6 @@
             out_buf[g][way[0], j, ch, e] = val.astype(BF16)
             partial_copy(ch, g, way, j, e).start()
 
-        for e in range(2):
-            sends.append((cond, functools.partial(partial_copy, ch, g, way, j, e)))
-
     outs, passed = (gu_ref, gd_ref), (yu, yd)
 
     def store(ch, g, e):
@@ -603,19 +598,19 @@
 
     def final_y(ch, g):
         return remote(
-            fin[g].at[ch, 0], passed[g].at[ch], fy_s.at[ch, g], fy_r.at[ch, g], ydev)
+            fin[g].at[ch, 0], passed[g].at[ch], out_s.at[7], fy_r.at[ch, g], ydev)
 
     def final_x(ch, g, e):
         src = passed[g].at[ch] if e else fin[g].at[ch, 1]
         i = (ch, g, e)
         return remote(
-            src, strip(g, outs[g], other if e else mine, ch), fx_s.at[i], fx_r.at[i], xdev)
+            src, strip(g, outs[g], other if e else mine, ch), out_s.at[7], fx_r.at[i], xdev)
 
     def final_x_in(ch, g, e):
         q = 2 * (1 - r) + (1 - y if e else y)
         src = passed[g].at[ch] if e else fin[g].at[ch, 1]
         i = (ch, g, e)
-        return remote(src, strip(g, outs[g], q, ch), fx_s.at[i], fx_r.at[i], xdev)
+        return remote(src, strip(g, outs[g], q, ch), out_s.at[7], fx_r.at[i], xdev)
 
     def finish(ch, g, m0, between=None):
         cond = level[m0]
@@ -627,44 +622,35 @@
                 val = val + in_buf[g][way[0], j, ch, e].astype(F32)
             fin[g][ch, e] = val.astype(BF16)
             if e == 0:
-                go(functools.partial(final_y, ch, g), cond)
+                go(functools.partial(final_y, ch, g))
                 if between:
                     between()
             else:
-                go(functools.partial(final_x, ch, g, 0), cond)
+                go(functools.partial(final_x, ch, g, 0))
         store(ch, g, 0).start()
 
     def spread(ch, g, m0):
         final_y(ch, g).wait_recv()
-        go(functools.partial(final_x, ch, g, 1), level[m0])
+        go(functools.partial(final_x, ch, g, 1))
         store(ch, g, 1).start()
-
-    h0 = isum0.shape[2]
-    cuts = ((0, h0), (h0, D))
-    isum, igot, ipt, ift = (isum0, isum1), (ira, irb), (ipt0, ipt1), (ift0, ift1)
 
     def ig_copy(i):
         if i == 0:
-            return remote(igp.at[1], itr, ig_s.at[0], ig_r.at[0], tdev)
-        if i > 6:
-            side, part = (i - 7) % 2, pl.ds((i - 7) // 2 * half, half)
-            src, dst = isum[side].at[1 + side, part, :], igot[side].at[0, part, :]
-            return remote(src, dst, ig_s.at[i], ig_r.at[i], (xdev, ydev)[side])
-        side, step = (i - 1) % 2, (i - 1) // 2
-        if step == 1:
-            src, dst = isum[side].at[3], igot[side].at[1]
+            return remote(igp.at[1], itr, out_s.at[8], ig_r.at[0], tdev)
+        kind, part = (i - 1) // 2, pl.ds((i - 1) % 2 * half, half)
+        if kind < 2:
+            src, dst = isum.at[3 - kind, part, :], igot.at[1 - kind, part, :]
         else:
-            src, dst = ipt[side], ift[side]
-        dev = (xdev, ydev)[side if step < 2 else 1 - side]
-        return remote(src, dst, ig_s.at[i], ig_r.at[i], dev)
-
-    def ig_go(i, cond):
-        go(functools.partial(ig_copy, i), cond)
-
-    def ig_part(cond):
+            src, dst = ipt.at[part, :], ift.at[part, :]
+        return remote(src, dst, out_s.at[8], ig_r.at[i], ydev if kind < 2 else xdev)
+
+    def ig_go(i):
+        go(functools.partial(ig_copy, i))
+
+    def ig_part():
         for dt in (1, 0):
 
-            @pl.loop(0, n, unroll=2)
+            @pl.loop(0, n, unroll=4)
             def _(b):
                 val = 0.0
                 for ch in range(C):
@@ -676,37 +662,33 @@
                     igp[dt, k, :, blk(b)] = val[k * tok:(k + 1) * tok]
 
             if dt:
-                ig_go(0, cond)
-
-    def ig_first(cond):
+                ig_go(0)
+
+    def ig_first():
         ig_copy(0).wait_recv()
 
         @pl.loop(0, 4)
         def _(k):
-            val = igp[0, k].astype(F32) + itr[k].astype(F32)
-            for side, (lo, hi) in enumerate(cuts):
-                isum[side][k] = val[:, lo:hi].astype(BF16)
-
-        for i in (4, 3):
-            ig_go(i, cond)
-
-    def ig_more(cond, part):
-        for side in range(2):
-            ig_go(7 + 2 * part + side, cond)
-
-    def ig_second(cond):
-        for side in range(2):
-            ig_copy(3 + side).wait_recv()
-            val = isum[side][2 - side].astype(F32) + igot[side][1].astype(F32)
-            ipt[side][...] = val.astype(BF16)
-            ig_go(5 + side, cond)
+            isum[k] = (igp[0, k].astype(F32) + itr[k].astype(F32)).astype(BF16)
+
+    def ig_diag(p):
+        ig_go(1 + p)
+
+    def ig_more(p):
+        ig_go(3 + p)
+
+    def ig_second(p):
+        ig_copy(1 + p).wait_recv()
+        part = pl.ds(p * half, half)
+        val = isum[1, part, :].astype(F32) + igot[1, part, :].astype(F32)
+        ipt[part, :] = val.astype(BF16)
+        ig_go(5 + p)
 
     def ig_last():
-        for side, (lo, hi) in enumerate(cuts):
-            for i in (5, 7, 9):
-                ig_copy(i + side).wait_recv()
-            val = isum[side][0].astype(F32) + igot[side][0].astype(F32)
-            igo[:, lo:hi] = (val + ift[side][...].astype(F32)).astype(BF16)
+        for i in range(3, 7):
+            ig_copy(i).wait_recv()
+        val = isum[0].astype(F32) + igot[0].astype(F32) + ift[...].astype(F32)
+        igo[...] = val.astype(BF16)
         store(C, 0, 0).start()
 
     edge, inner = level[0], m > 0
@@ -723,7 +705,7 @@
         start("x", "x", i)
         start("y", "x", i)
     loads["mine", 0, 1].wait()
-    begin(0, 1, 0, edge)
+    begin(0, 1, 0)
     start("s", "x", 0)
     loads["c"].wait()
     start("s", "c", 0)
@@ -745,16 +727,19 @@
     start("d", "x", 0)
     for k in range(2, Z - 1):
         relay(0, 0, k)
-    for unit in units[1:3]:
+    for unit in units[2:3]:
         begin(*unit, 0, inner)
     for i in range(2):
         arrive("x", "x", i)
     start("s", "x", 1)
     arrive("y", "x", 1)
     start("d", "x", 1)
-    for i in range(min(2, Z)):
-        start("x", "c", i)
-        start("y", "c", i)
+
+    def offer(i):
+        for way in ("x0", "y0", "x1", "y1"):
+            start(way, "c", i)
+
+    offer(0)
     start("s", "x", 2)
     swap(0, 1).wait_recv()
     begin(0, 1, 1)
@@ -783,15 +768,12 @@
 
     tasks = [(unit, k) for unit in units[2:] for k in range(1, Z - 1)]
     for i in range(Z):
-        arrive("x", "c", i)
+        arrive("x0", "c", i)
         start("dy", "c", i)
-        start("s1", "c", i)
-        arrive("y", "c", i)
+        arrive("y0", "c", i)
         start("dx", "c", i)
-        start("s2", "c", i)
-        if i + 2 < Z:
-            start("x", "c", i + 2)
-            start("y", "c", i + 2)
+        if i + 1 < Z:
+            offer(i + 1)
         if i == 0:
             for k in range(2, Z - 1):
                 relay(0, 1, k, (1,))
@@ -806,40 +788,31 @@
             flip(3)
             forward(0, 3, 4)
         else:
-            ready(i - 1)
+            if i > 1:
+                ready(i - 1)
             if i == Z - 1:
                 for m0 in range(1, Z // 2):
                     pl.when(level[m0])(functools.partial(reduce, 0, 1, near, 0, m0))
+        arrive("x1", "c", i)
+        start("s1", "c", i)
+        arrive("y1", "c", i)
+        start("s2", "c", i)
         arrive("dy", "c", i)
         arrive("dx", "c", i)
         start("s3", "c", i)
+        if i == 0:
+            ready(0)
         if i == 1 and tasks:
             unit, k = tasks.pop(0)
             relay(*unit, k, toward=1)
-    ready(Z - 1)
-
-    early = list(sends)
-    sends.clear()
-
-    def drain(some):
-        for cond, make in some:
-            if cond is None:
-                make().wait_send()
-            else:
-                pl.when(cond)(lambda: make().wait_send())
-
-    def flush(base, count):
-        some = sends[base:count]
-        del sends[base:count]
-        drain(some)
+    if Z > 1:
+        ready(Z - 1)
 
     def edges():
-        base = len(sends)
         collect(0, 1)
         backward(0)
         for j in range(Z - 1):
             reduce(0, 0, near, j, 0)
-        drain(early)
         for ch in range(1, C):
             collect(ch, 0)
             forward(ch, 0, 4)
@@ -850,35 +823,34 @@
             if ch < C - 1:
                 for j in range(Z - 1):
                     reduce(ch, 0, near, j, 0)
-        count = len(sends)
-        ig_part(edge)
+        ig_part()
         finish(0, 1, 0)
-        ig_first(edge)
+        ig_first()
+        ig_diag(0)
         if C > 1:
             for j in range(Z - 1):
                 reduce(C - 1, 0, near, j, 0)
         finish(0, 0, 0)
+        ig_diag(1)
         spread(0, 1, 0)
+        ig_second(0)
         for ch in range(1, C):
             finish(ch, 1, 0)
-            if ch == 1:
-                ig_second(edge)
             spread(ch - 1, 0, 0)
             if ch == 1:
-                ig_more(edge, 0)
-                flush(base, count)
+                ig_more(0)
+                ig_second(1)
             finish(ch, 0, 0, lambda: spread(ch, 1, 0))
             if ch == 1:
-                ig_more(edge, 1)
+                ig_more(1)
         if C == 1:
-            ig_second(edge)
-            ig_more(edge, 0)
-            ig_more(edge, 1)
+            ig_more(0)
+            ig_second(1)
+            ig_more(1)
         spread(C - 1, 0, 0)
         ig_last()
 
     def inside(m0):
-        cond, base = level[m0], len(sends)
         left = list(tasks)
 
         def relays(count):
@@ -911,35 +883,36 @@
         nears(0, 0, rest)
         spread(0, 1, m0)
         fars(0, 0)
-        ig_part(cond)
-        drain(early)
+        ig_part()
         finish(0, 0, m0)
         for ch in range(1, C):
             nears(ch, 1, first)
             if ch == 1:
-                ig_first(cond)
+                ig_first()
+                ig_diag(0)
+                ig_diag(1)
             spread(ch - 1, 0, m0)
-            if ch == 1:
-                ig_more(cond, 0)
             nears(ch, 1, rest)
             fars(ch, 1)
             if ch == 1:
-                ig_second(cond)
+                ig_second(0)
             finish(ch, 1, m0)
-            count = len(sends)
-            nears(ch, 0, (0, *rest))
+            nears(ch, 0, first)
+            if ch == 1:
+                ig_more(0)
+                ig_second(1)
+                ig_more(1)
+            nears(ch, 0, rest)
             fars(ch, 0)
-            if ch == 1:
-                ig_more(cond, 1)
             spread(ch, 1, m0)
-            if ch == C - 1:
-                flush(base, count)
             finish(ch, 0, m0)
         if C == 1:
-            ig_first(cond)
-            ig_more(cond, 0)
-            ig_more(cond, 1)
-            ig_second(cond)
+            ig_first()
+            for p in range(2):
+                ig_diag(p)
+                ig_more(p)
+            for p in range(2):
+                ig_second(p)
         spread(C - 1, 0, m0)
         ig_last()
 
@@ -955,8 +928,25 @@
                     store(ch, g, e).wait()
         store(C, 0, 0).wait()
 
+    def sent(i, count):
+        some = xg.at[pl.ds(0, count), :]
+        remote(some, some, out_s.at[i], out_s.at[i], xdev).wait_send()
+
+    def drain():
+        block = 4 * hw // n
+        sent(0, block // 2)
+        for z0 in range(Z - 1):
+            pl.when(z == z0)(functools.partial(sent, 1, (z0 + 1) * block))
+            pl.when(z == Z - 1 - z0)(functools.partial(sent, 2, (z0 + 1) * block))
+        sent(3, 7 * half)
+        sent(4, 5 * half)
+        sent(5, 8 * tok)
+        sent(6, (Z - 1) * block)
+        sent(7, 3 * block // 2)
+        sent(8, 7 * tok)
+
     settle()
-    drain(sends)
+    drain()
 
 
 def ring_call(inputs, up_weight):
@@ -986,6 +976,34 @@
     return functools.partial(ring_kernel, R, n, T), scratch, (R, hb), pltpu.VMEM
 
 
+def finals_kernel(scale, ig, gu, gd, ig_out, gu_out, gd_out):
+    ig_out[...] = ig[...]
+    gu_out[...] = gu[...].astype(F32) * scale
+    gd_out[...] = gd[...].astype(F32) * scale
+
+
+def finals_call(ig, gu, gd, scale):
+    steps = 4
+    tok, D = ig.shape
+    db, HB = gu.shape
+    specs = [
+        pl.BlockSpec((tok // steps, D), lambda i: (i, 0)),
+        pl.BlockSpec((db // steps, HB), lambda i: (i, 0)),
+        pl.BlockSpec((HB // steps, db), lambda i: (i, 0)),
+    ]
+    return pl.pallas_call(
+        functools.partial(finals_kernel, scale),
+        grid=(steps,),
+        in_specs=specs,
+        out_specs=specs,
+        out_shape=(
+            jax.ShapeDtypeStruct(ig.shape, BF16),
+            jax.ShapeDtypeStruct(gu.shape, F32),
+            jax.ShapeDtypeStruct(gd.shape, F32),
+        ),
+    )(ig, gu, gd)
+
+
 def axis_sizes():
     return lax.axis_size("rep"), lax.axis_size("fs"), lax.axis_size("tp")
 
@@ -995,21 +1013,19 @@
     tok, D = inputs.shape
     db, HB = up_weight.shape
     Z, G = n // 2, 2 * R
-    if R != 2 or T != 2 or n % 4 or tok % 32 or HB % (128 * G) or db % 128 or D % 1024:
+    if R != 2 or T != 2 or n % 4 or tok % 32 or HB % (128 * G) or db % 128:
         return None
     hw = HB // G
     C = tile_of(hw // 128, CHUNKS)
     hc = hw // C
-    rows, h0 = 8 * tok, D // 8
-    h1 = D - h0
+    rows = 8 * tok
     V, S = pltpu.VMEM, pltpu.SemaphoreType.DMA
     data = [
         ((rows, D), BF16), ((rows, D), BF16), ((D, rows), BF16),
         ((C, D, hc), BF16), ((C, hc, D), BF16),
         ((C, rows, hc), F32), ((C, rows, hc), BF16), ((C, hc, rows), BF16),
-        ((2, 4, tok, D), BF16), ((4, tok, D), BF16), ((4, tok, h0), BF16), ((4, tok, h1), BF16),
-        ((2, tok, h0), BF16), ((2, tok, h1), BF16), ((tok, h0), BF16), ((tok, h1), BF16),
-        ((tok, h0), BF16), ((tok, h1), BF16),
+        ((2, 4, tok, D), BF16), ((4, tok, D), BF16), ((4, tok, D), BF16),
+        ((2, tok, D), BF16), ((tok, D), BF16), ((tok, D), BF16),
         ((tok, D), BF16),
         ((2, Z - 1, C, 2, db, hc), BF16), ((2, Z - 1, C, 2, hc, db), BF16),
         ((2, Z - 1, C, 2, db, hc), BF16), ((2, Z - 1, C, 2, hc, db), BF16),
@@ -1017,13 +1033,13 @@
         ((C, db, hc), BF16), ((C, hc, db), BF16), ((C, db, hc), BF16), ((C, hc, db), BF16),
     ]
     size = sum(math.prod(s) * jnp.dtype(d).itemsize for s, d in data)
-    if size > 50 * 2**20:
+    if size > 50 * 2**20 or 4 * hw % n or (Z - 1) * 4 * hw > 8 * tok * n:
         return None
     sems = [
-        (C, 2), (C, 2, Z - 1, 2, 2), (4 + 2 * Z,), (2 + 2 * Z,), (5 + 3 * Z,),
-        (2, Z - 1, C, 2, 2), (C, 2), (C, 2, 2), (11,),
+        (C, 2), (C, 2, Z - 1, 2, 2), (4 + 3 * Z,), (2 + 3 * Z,), (5 + 3 * Z,),
+        (2, Z - 1, C, 2, 2), (C, 2), (C, 2, 2), (7,),
     ]
-    scratch = [V(s, d) for s, d in data] + [S(s) for s in sems for _ in range(2)]
+    scratch = [V(s, d) for s, d in data] + [S((9,))] + [S(s) for s in sems]
     scratch += [S((4 * C + 2,)), S((4 * C + 1,))]
     return functools.partial(plane_kernel, Z), scratch, (1, HB), pl.ANY
 
@@ -1051,6 +1067,8 @@
     )(inputs, cotangent, up_weight, down_weight)
     total_tokens = tok * R * n * T
     loss_scale = 1.0 / math.sqrt(total_tokens)
+    if space is pl.ANY:
+        return finals_call(ig, gu, gd, loss_scale)
     return ig, gu.astype(F32) * loss_scale, gd.astype(F32) * loss_scale
 
 

time: 131 us -> 125 us (0.954)
  other arithmetic: 4.33 us -> 0 us
    pallas_call x1, Pallas kernels: 125 us -> 120 us  [shards(): pl.pallas_call(body, out_shape=(jax.ShapeDtypeStruct((tok, D), BF16), jax...]
    pallas_call x0 -> x1, Pallas kernels: none -> 4.36 us  [finals_call(): pl.pallas_call(functools.partial(finals_kernel, scale), grid=(steps,), in...]
    mul x2 -> x0, other arithmetic: 4.33 us -> none  [shards(): return (ig, gu.astype(F32) * loss_scale, gd.astype(F32) * loss_scale)]
where the time goes in v3:
time: 125 us
  Pallas kernels  124 us (99%)
    pallas_call x1, Pallas kernels, shards(): pl.pallas_call(body, out_shape=(jax.ShapeDtypeStruct((tok, D), BF16), jax...  120 us
    pallas_call x1, Pallas kernels, finals_call(): pl.pallas_call(functools.partial(finals_kernel, scale), grid=(steps,), in...  4.36 us

profile of v3, /device:TPU:0, one launch (start us, length us, event | category | flops | bytes accessed | tf_op | source)
XLA Modules:
  0.0 125.0 jit_solution(15034664382434024497)
XLA Ops:
  0.6 120.0 %shard_map.67 = (bf16[128,2048]{1,0:T(8,128)(2,1)}, bf16[256,2048]{1,0:T(8,128)(2,1)}, bf16[2048,256]{1,0:T(8,128)(2,1)}) custom-call(bf16[128,2048]{1,0:T(8,128)(2,1)} %x_ref.1, bf16[128,2048]{1,0:T(8,128)(2,1)} %c_ref.1, bf16[256,2048]{1,0:T(8,128)(2,1)} %u_ref.1, bf16[2048,256]{1,0:T(8,128)(2,1)} %d_ref.1), custom_call_target="tpu_custom_call" | custom-call | tf_op jit(solution)/shard_map/pallas_call | solution.py:1054
  120.6 4.4 %shard_map.68 = (bf16[128,2048]{1,0:T(8,128)(2,1)}, f32[256,2048]{1,0:T(8,128)}, f32[2048,256]{1,0:T(8,128)}) custom-call(bf16[128,2048]{1,0:T(8,128)(2,1)} %get-tuple-element.6.ig, bf16[256,2048]{1,0:T(8,128)(2,1)} %get-tuple-element.7.gu, bf16[2048,256]{1,0:T(8,128)(2,1)} %get-tuple-element.8.gd), custom_call_target="tpu_custom_call" | custom-call | tf_op jit(solution)/shard_map/pallas_call | solution.py:994

commit v4 on v3

--- a/solution.py
+++ b/solution.py
@@ -10,6 +10,7 @@
 
 MESH = pl.DeviceIdType.MESH
 CHUNKS = 2
+PARTS = 4
 BF16, F32 = jnp.bfloat16, jnp.float32
 NT = (((1,), (1,)), ((), ()))
 
@@ -573,13 +574,12 @@
     def side_of(e):
         return e * y + (1 - e) * (1 - y)
 
-    def reduce(ch, g, way, j, m0):
+    def reduce(ch, g, way, j, m0, es=None):
         cond = level[m0]
         to = jnp.where(way[1] > 0, Z - 1 - j, j)
         more = m0 > 0 or way is far
 
-        @pl.loop(0, 2)
-        def _(e):
+        def step(e):
             val = grad(ch, g, 2 * to + side_of(e))
             if more:
                 partial_copy(ch, g, way, j, e).wait_recv()
@@ -587,14 +587,20 @@
             out_buf[g][way[0], j, ch, e] = val.astype(BF16)
             partial_copy(ch, g, way, j, e).start()
 
+        if es is None:
+            pl.loop(0, 2)(step)
+        else:
+            for e in es:
+                step(e)
+
     outs, passed = (gu_ref, gd_ref), (yu, yd)
 
     def store(ch, g, e):
         if ch == C:
-            return pltpu.make_async_copy(igo, ig_ref, st_s.at[4 * C])
+            return pltpu.make_async_copy(igo, ig_ref, st_s.at[1])
         src = passed[g].at[ch] if e else fin[g].at[ch, 1]
         dst = strip(g, outs[g], other if e else mine, ch)
-        return pltpu.make_async_copy(src, dst, st_s.at[4 * ch + 2 * g + e])
+        return pltpu.make_async_copy(src, dst, st_s.at[0])
 
     def final_y(ch, g):
         return remote(
@@ -602,15 +608,8 @@
 
     def final_x(ch, g, e):
         src = passed[g].at[ch] if e else fin[g].at[ch, 1]
-        i = (ch, g, e)
         return remote(
-            src, strip(g, outs[g], other if e else mine, ch), out_s.at[7], fx_r.at[i], xdev)
-
-    def final_x_in(ch, g, e):
-        q = 2 * (1 - r) + (1 - y if e else y)
-        src = passed[g].at[ch] if e else fin[g].at[ch, 1]
-        i = (ch, g, e)
-        return remote(src, strip(g, outs[g], q, ch), out_s.at[7], fx_r.at[i], xdev)
+            src, strip(g, outs[g], other if e else mine, ch), out_s.at[7], fx_r.at[0], xdev)
 
     def finish(ch, g, m0, between=None):
         cond = level[m0]
@@ -634,42 +633,47 @@
         go(functools.partial(final_x, ch, g, 1))
         store(ch, g, 1).start()
 
+    def cols(p):
+        return pl.ds(p * (D // 2), D // 2)
+
     def ig_copy(i):
-        if i == 0:
-            return remote(igp.at[1], itr, out_s.at[8], ig_r.at[0], tdev)
-        kind, part = (i - 1) // 2, pl.ds((i - 1) % 2 * half, half)
+        part = cols((i + 1) % 2)
+        if i > 6:
+            part = cols(i - 7)
+            src, dst = igp.at[1, :, :, part], itr.at[:, :, part]
+            return remote(src, dst, out_s.at[8], ig_r.at[i - 1], tdev)
+        kind = (i - 1) // 2
         if kind < 2:
-            src, dst = isum.at[3 - kind, part, :], igot.at[1 - kind, part, :]
+            src, dst = isum.at[3 - kind, :, part], igot.at[1 - kind, :, part]
         else:
-            src, dst = ipt.at[part, :], ift.at[part, :]
-        return remote(src, dst, out_s.at[8], ig_r.at[i], ydev if kind < 2 else xdev)
+            src, dst = ipt.at[:, part], ift.at[:, part]
+        return remote(src, dst, out_s.at[8], ig_r.at[i - 1], ydev if kind < 2 else xdev)
 
     def ig_go(i):
         go(functools.partial(ig_copy, i))
 
-    def ig_part():
-        for dt in (1, 0):
-
-            @pl.loop(0, n, unroll=4)
-            def _(b):
-                val = 0.0
-                for ch in range(C):
-                    lhs = jnp.concatenate([pg[ch, rows(k, dt), :] for k in range(4)], 0)
-                    val = val + lax.dot_general(
-                        lhs, ug[ch, blk(b), :], NT, preferred_element_type=F32)
-                val = val.astype(BF16)
-                for k in range(4):
-                    igp[dt, k, :, blk(b)] = val[k * tok:(k + 1) * tok]
-
-            if dt:
-                ig_go(0)
-
-    def ig_first():
-        ig_copy(0).wait_recv()
+    def ig_part(dt, p):
+        @pl.loop(p * (n // 2), (p + 1) * (n // 2), unroll=n // 2)
+        def _(b):
+            val = 0.0
+            for ch in range(C):
+                lhs = jnp.concatenate([pg[ch, rows(k, dt), :] for k in range(4)], 0)
+                val = val + lax.dot_general(
+                    lhs, ug[ch, blk(b), :], NT, preferred_element_type=F32)
+            val = val.astype(BF16)
+            for k in range(4):
+                igp[dt, k, :, blk(b)] = val[k * tok:(k + 1) * tok]
+
+        if dt:
+            ig_go(7 + p)
+
+    def ig_first(p):
+        ig_copy(7 + p).wait_recv()
 
         @pl.loop(0, 4)
         def _(k):
-            isum[k] = (igp[0, k].astype(F32) + itr[k].astype(F32)).astype(BF16)
+            val = igp[0, k, :, cols(p)].astype(F32) + itr[k, :, cols(p)].astype(F32)
+            isum[k, :, cols(p)] = val.astype(BF16)
 
     def ig_diag(p):
         ig_go(1 + p)
@@ -679,9 +683,8 @@
 
     def ig_second(p):
         ig_copy(1 + p).wait_recv()
-        part = pl.ds(p * half, half)
-        val = isum[1, part, :].astype(F32) + igot[1, part, :].astype(F32)
-        ipt[part, :] = val.astype(BF16)
+        val = isum[1, :, cols(p)].astype(F32) + igot[1, :, cols(p)].astype(F32)
+        ipt[:, cols(p)] = val.astype(BF16)
         ig_go(5 + p)
 
     def ig_last():
@@ -823,16 +826,23 @@
             if ch < C - 1:
                 for j in range(Z - 1):
                     reduce(ch, 0, near, j, 0)
-        ig_part()
-        finish(0, 1, 0)
-        ig_first()
-        ig_diag(0)
+        ig_part(1, 0)
+        ig_part(1, 1)
+
+        def meanwhile():
+            ig_part(0, 0)
+            ig_first(0)
+            ig_diag(0)
+            ig_part(0, 1)
+
+        finish(0, 1, 0, meanwhile)
+        ig_first(1)
         if C > 1:
             for j in range(Z - 1):
                 reduce(C - 1, 0, near, j, 0)
-        finish(0, 0, 0)
         ig_diag(1)
         spread(0, 1, 0)
+        finish(0, 0, 0)
         ig_second(0)
         for ch in range(1, C):
             finish(ch, 1, 0)
@@ -840,7 +850,8 @@
             if ch == 1:
                 ig_more(0)
                 ig_second(1)
-            finish(ch, 0, 0, lambda: spread(ch, 1, 0))
+            spread(ch, 1, 0)
+            finish(ch, 0, 0)
             if ch == 1:
                 ig_more(1)
         if C == 1:
@@ -865,6 +876,13 @@
         def fars(ch, g):
             for j in range(m0):
                 reduce(ch, g, far, j, m0)
+
+        def both(ch, g):
+            for e in range(2):
+                for j in range(m0):
+                    reduce(ch, g, far, j, m0, (e,))
+                for j in rest:
+                    reduce(ch, g, near, j, m0, (e,))
 
         first, rest = range(1), range(1, Z - 1 - m0)
         keep = (Z - 2) * (C > 1)
@@ -880,20 +898,20 @@
             backward(ch)
         nears(0, 0, first)
         finish(0, 1, m0)
-        nears(0, 0, rest)
+        both(0, 0)
         spread(0, 1, m0)
-        fars(0, 0)
-        ig_part()
+        for dt in (1, 0):
+            for p in range(2):
+                ig_part(dt, p)
         finish(0, 0, m0)
         for ch in range(1, C):
             nears(ch, 1, first)
             if ch == 1:
-                ig_first()
-                ig_diag(0)
-                ig_diag(1)
+                for p in range(2):
+                    ig_first(p)
+                    ig_diag(p)
             spread(ch - 1, 0, m0)
-            nears(ch, 1, rest)
-            fars(ch, 1)
+            both(ch, 1)
             if ch == 1:
                 ig_second(0)
             finish(ch, 1, m0)
@@ -902,13 +920,12 @@
                 ig_more(0)
                 ig_second(1)
                 ig_more(1)
-            nears(ch, 0, rest)
-            fars(ch, 0)
+            both(ch, 0)
             spread(ch, 1, m0)
             finish(ch, 0, m0)
         if C == 1:
-            ig_first()
             for p in range(2):
+                ig_first(p)
                 ig_diag(p)
                 ig_more(p)
             for p in range(2):
@@ -921,11 +938,8 @@
         pl.when(level[m0])(functools.partial(inside, m0))
 
     def settle():
-        for ch in range(C):
-            for g in (1, 0):
-                for e in range(2):
-                    final_x_in(ch, g, e).wait_recv()
-                    store(ch, g, e).wait()
+        remote(gu_ref, gu_ref, out_s.at[7], fx_r.at[0], xdev).wait_recv()
+        pltpu.make_async_copy(gu_ref, gu_ref, st_s.at[0]).wait()
         store(C, 0, 0).wait()
 
     def sent(i, count):
@@ -976,31 +990,51 @@
     return functools.partial(ring_kernel, R, n, T), scratch, (R, hb), pltpu.VMEM
 
 
-def finals_kernel(scale, ig, gu, gd, ig_out, gu_out, gd_out):
-    ig_out[...] = ig[...]
-    gu_out[...] = gu[...].astype(F32) * scale
-    gd_out[...] = gd[...].astype(F32) * scale
+def finals_kernel(scale, *refs):
+    sources, targets, raw, wide = refs[:3], refs[3:6], refs[6:9], refs[9:11]
+    load, store = refs[11:]
+    jobs = []
+    for a in (1, 2, 0):
+        rows = sources[a].shape[0]
+        for p in range(PARTS):
+            part = pl.ds(p * (rows // PARTS), rows // PARTS)
+            jobs.append((a, p, part))
+    loads, stores = [], []
+    for a, p, part in jobs:
+        copy = pltpu.make_async_copy(
+            sources[a].at[part, :], raw[a].at[part, :], load.at[a, p])
+        copy.start()
+        loads.append(copy)
+    for (a, p, part), copy in zip(jobs, loads):
+        copy.wait()
+        ready = raw[a]
+        if a:
+            ready = wide[a - 1]
+            ready[part, :] = raw[a][part, :].astype(F32) * scale
+        copy = pltpu.make_async_copy(
+            ready.at[part, :], targets[a].at[part, :], store.at[a, p])
+        copy.start()
+        stores.append(copy)
+    for copy in stores:
+        copy.wait()
 
 
 def finals_call(ig, gu, gd, scale):
-    steps = 4
-    tok, D = ig.shape
-    db, HB = gu.shape
-    specs = [
-        pl.BlockSpec((tok // steps, D), lambda i: (i, 0)),
-        pl.BlockSpec((db // steps, HB), lambda i: (i, 0)),
-        pl.BlockSpec((HB // steps, db), lambda i: (i, 0)),
-    ]
+    any_space = pl.BlockSpec(memory_space=pl.ANY)
+    V, S = pltpu.VMEM, pltpu.SemaphoreType.DMA
     return pl.pallas_call(
         functools.partial(finals_kernel, scale),
-        grid=(steps,),
-        in_specs=specs,
-        out_specs=specs,
+        in_specs=[any_space] * 3,
+        out_specs=(any_space,) * 3,
         out_shape=(
             jax.ShapeDtypeStruct(ig.shape, BF16),
             jax.ShapeDtypeStruct(gu.shape, F32),
             jax.ShapeDtypeStruct(gd.shape, F32),
         ),
+        scratch_shapes=[
+            V(ig.shape, BF16), V(gu.shape, BF16), V(gd.shape, BF16),
+            V(gu.shape, F32), V(gd.shape, F32), S((3, PARTS)), S((3, PARTS)),
+        ],
     )(ig, gu, gd)
 
 
@@ -1037,10 +1071,10 @@
         return None
     sems = [
         (C, 2), (C, 2, Z - 1, 2, 2), (4 + 3 * Z,), (2 + 3 * Z,), (5 + 3 * Z,),
-        (2, Z - 1, C, 2, 2), (C, 2), (C, 2, 2), (7,),
+        (2, Z - 1, C, 2, 2), (C, 2), (1,), (8,),
     ]
     scratch = [V(s, d) for s, d in data] + [S((9,))] + [S(s) for s in sems]
-    scratch += [S((4 * C + 2,)), S((4 * C + 1,))]
+    scratch += [S((4 * C + 2,)), S((2,))]
     return functools.partial(plane_kernel, Z), scratch, (1, HB), pl.ANY
 
 

time: 125 us -> 123 us (0.984)
  Pallas kernels: 124 us -> 122 us
    pallas_call x1, Pallas kernels: 120 us -> 118 us  [shards(): pl.pallas_call(body, out_shape=(jax.ShapeDtypeStruct((tok, D), BF16), jax...]
where the time goes in v4:
time: 123 us
  Pallas kernels  122 us (99%)
    pallas_call x1, Pallas kernels, shards(): pl.pallas_call(body, out_shape=(jax.ShapeDtypeStruct((tok, D), BF16), jax...  118 us
    pallas_call x1, Pallas kernels, finals_call(): pl.pallas_call(functools.partial(finals_kernel, scale), in_specs=[any_spa...  3.35 us

profile of v4, /device:TPU:0, one launch (start us, length us, event | category | flops | bytes accessed | tf_op | source)
XLA Modules:
  0.0 122.6 jit_solution(5135187678599993226)
XLA Ops:
  0.6 118.5 %shard_map.67 = (bf16[128,2048]{1,0:T(8,128)(2,1)}, bf16[256,2048]{1,0:T(8,128)(2,1)}, bf16[2048,256]{1,0:T(8,128)(2,1)}) custom-call(bf16[128,2048]{1,0:T(8,128)(2,1)} %x_ref.1, bf16[128,2048]{1,0:T(8,128)(2,1)} %c_ref.1, bf16[256,2048]{1,0:T(8,128)(2,1)} %u_ref.1, bf16[2048,256]{1,0:T(8,128)(2,1)} %d_ref.1), custom_call_target="tpu_custom_call" | custom-call | tf_op jit(solution)/shard_map/pallas_call | solution.py:1088
  119.1 3.3 %shard_map.68 = (bf16[128,2048]{1,0:T(8,128)(2,1)}, f32[256,2048]{1,0:T(8,128)}, f32[2048,256]{1,0:T(8,128)}) custom-call(bf16[128,2048]{1,0:T(8,128)(2,1)} %get-tuple-element.6.refs_0_, bf16[256,2048]{1,0:T(8,128)(2,1)} %get-tuple-element.7.refs_1_, bf16[2048,256]{1,0:T(8,128)(2,1)} %get-tuple-element.8.refs_2_), custom_call_target="tpu_custom_call" | custom-call | tf_op jit(solution)/shard_map/pallas_call | solution.py:1025

commit v5 on v4

--- a/solution.py
+++ b/solution.py
@@ -442,13 +442,13 @@
 
     def pass_on(ch, g, s, k, e):
         block = held(g, ch, origin(s, k, e))
-        i = (ch, (1 - s) // 2, k, e, g)
-        return remote(block, block, out_s.at[i[1] + 1], zg_r.at[i], zdev(s))
+        i = (ch, z - s * k, e, g)
+        return remote(block, block, out_s.at[(3 - s) // 2], zg_r.at[i], zdev(s))
 
     def landed(ch, g, s, k, e):
         block = held(g, ch, origin(s, k, e))
-        i = (ch, (1 - s) // 2, k - 1, e, g)
-        return remote(block, block, out_s.at[i[1] + 1], zg_r.at[i], zdev(s))
+        i = (ch, z - s * k, e, g)
+        return remote(block, block, out_s.at[(3 - s) // 2], zg_r.at[i], zdev(s))
 
     def begin(ch, g, e, also=None):
         for s in (1, -1):
@@ -527,7 +527,7 @@
         moves["dy", "c", i] = hop(Y, 4 + 3 * i, ydev, cg, (1, 0, B), (3, 0, B), i)
         for k in range(1, 4):
             moves["s%d" % k, "c", i] = hop(
-                S, 5 + (k - 1) * Z + i, tdev, cg, (k, 0, AB), (k, 1, AB), i)
+                S, 5 + i, tdev, cg, (k, 0, AB), (k, 1, AB), i)
 
     def start(*key):
         go(moves[key])
@@ -764,8 +764,8 @@
     start("s", "x", 3)
 
     def ready(i):
-        for k in range(1, 4):
-            arrive("s%d" % k, "c", i)
+        three = cg.at[pl.ds(0, 3 * tok), quarter(i)]
+        remote(three, three, out_s.at[5], tt_r.at[5 + i], tdev).wait_recv()
         if i < Z - 1:
             pl.when(edge)(functools.partial(reduce, 0, 1, near, i, 0))
 
@@ -914,8 +914,9 @@
             both(ch, 1)
             if ch == 1:
                 ig_second(0)
+            reduce(ch, 0, near, 0, m0, (0,))
             finish(ch, 1, m0)
-            nears(ch, 0, first)
+            reduce(ch, 0, near, 0, m0, (1,))
             if ch == 1:
                 ig_more(0)
                 ig_second(1)
@@ -1070,7 +1071,7 @@
     if size > 50 * 2**20 or 4 * hw % n or (Z - 1) * 4 * hw > 8 * tok * n:
         return None
     sems = [
-        (C, 2), (C, 2, Z - 1, 2, 2), (4 + 3 * Z,), (2 + 3 * Z,), (5 + 3 * Z,),
+        (C, 2), (C, Z, 2, 2), (4 + 3 * Z,), (2 + 3 * Z,), (5 + Z,),
         (2, Z - 1, C, 2, 2), (C, 2), (1,), (8,),
     ]
     scratch = [V(s, d) for s, d in data] + [S((9,))] + [S(s) for s in sems]

time: 123 us -> 123 us (level)
  no operation moved by 1% of the time
where the time goes in v5:
time: 123 us; the launch traced here: 122 us
  Pallas kernels  122 us (99%)
    pallas_call x1, Pallas kernels, shards(): pl.pallas_call(body, out_shape=(jax.ShapeDtypeStruct((tok, D), BF16), jax...  118 us
    pallas_call x1, Pallas kernels, finals_call(): pl.pallas_call(functools.partial(finals_kernel, scale), in_specs=[any_spa...  3.35 us

profile of v5, /device:TPU:0, one launch (start us, length us, event | category | flops | bytes accessed | tf_op | source)
XLA Modules:
  0.0 122.4 jit_solution(10233643963400584341)
XLA Ops:
  0.6 118.3 %shard_map.67 = (bf16[128,2048]{1,0:T(8,128)(2,1)}, bf16[256,2048]{1,0:T(8,128)(2,1)}, bf16[2048,256]{1,0:T(8,128)(2,1)}) custom-call(bf16[128,2048]{1,0:T(8,128)(2,1)} %x_ref.1, bf16[128,2048]{1,0:T(8,128)(2,1)} %c_ref.1, bf16[256,2048]{1,0:T(8,128)(2,1)} %u_ref.1, bf16[2048,256]{1,0:T(8,128)(2,1)} %d_ref.1), custom_call_target="tpu_custom_call" | custom-call | tf_op jit(solution)/shard_map/pallas_call | solution.py:1089
  118.9 3.3 %shard_map.68 = (bf16[128,2048]{1,0:T(8,128)(2,1)}, f32[256,2048]{1,0:T(8,128)}, f32[2048,256]{1,0:T(8,128)}) custom-call(bf16[128,2048]{1,0:T(8,128)(2,1)} %get-tuple-element.6.refs_0_, bf16[256,2048]{1,0:T(8,128)(2,1)} %get-tuple-element.7.refs_1_, bf16[2048,256]{1,0:T(8,128)(2,1)} %get-tuple-element.8.refs_2_), custom_call_target="tpu_custom_call" | custom-call | tf_op jit(solution)/shard_map/pallas_call | solution.py:1026

commit v6 on v5

--- a/solution.py
+++ b/solution.py
@@ -569,7 +569,7 @@
         d, s = way
         return remote(
             out_buf[g].at[d, j, ch, e], in_buf[g].at[d, j, ch, e],
-            out_s.at[6], rs_r.at[d, j, ch, g, e], zdev(s))
+            out_s.at[6], rs_r.at[j + d * (Z - 2 * j), ch, g, e], zdev(s))
 
     def side_of(e):
         return e * y + (1 - e) * (1 - y)
@@ -1000,7 +1000,7 @@
         for p in range(PARTS):
             part = pl.ds(p * (rows // PARTS), rows // PARTS)
             jobs.append((a, p, part))
-    loads, stores = [], []
+    loads = []
     for a, p, part in jobs:
         copy = pltpu.make_async_copy(
             sources[a].at[part, :], raw[a].at[part, :], load.at[a, p])
@@ -1013,11 +1013,11 @@
             ready = wide[a - 1]
             ready[part, :] = raw[a][part, :].astype(F32) * scale
         copy = pltpu.make_async_copy(
-            ready.at[part, :], targets[a].at[part, :], store.at[a, p])
+            ready.at[part, :], targets[a].at[part, :], store.at[a])
         copy.start()
-        stores.append(copy)
-    for copy in stores:
-        copy.wait()
+    for a in range(3):
+        whole = wide[a - 1] if a else raw[a]
+        pltpu.make_async_copy(whole, targets[a], store.at[a]).wait()
 
 
 def finals_call(ig, gu, gd, scale):
@@ -1034,7 +1034,7 @@
         ),
         scratch_shapes=[
             V(ig.shape, BF16), V(gu.shape, BF16), V(gd.shape, BF16),
-            V(gu.shape, F32), V(gd.shape, F32), S((3, PARTS)), S((3, PARTS)),
+            V(gu.shape, F32), V(gd.shape, F32), S((3, PARTS)), S((3,)),
         ],
     )(ig, gu, gd)
 
@@ -1072,7 +1072,7 @@
         return None
     sems = [
         (C, 2), (C, Z, 2, 2), (4 + 3 * Z,), (2 + 3 * Z,), (5 + Z,),
-        (2, Z - 1, C, 2, 2), (C, 2), (1,), (8,),
+        (Z + 1, C, 2, 2), (C, 2), (1,), (8,),
     ]
     scratch = [V(s, d) for s, d in data] + [S((9,))] + [S(s) for s in sems]
     scratch += [S((4 * C + 2,)), S((2,))]

time: 123 us -> 122 us (level)
  no operation moved by 1% of the time
where the time goes in v6:
time: 122 us
  Pallas kernels  121 us (99%)
    pallas_call x1, Pallas kernels, shards(): pl.pallas_call(body, out_shape=(jax.ShapeDtypeStruct((tok, D), BF16), jax...  118 us
    pallas_call x1, Pallas kernels, finals_call(): pl.pallas_call(functools.partial(finals_kernel, scale), in_specs=[any_spa...  3.27 us

profile of v6, /device:TPU:0, one launch (start us, length us, event | category | flops | bytes accessed | tf_op | source)
XLA Modules:
  0.0 122.3 jit_solution(6563391839277734522)
XLA Ops:
  0.6 118.2 %shard_map.67 = (bf16[128,2048]{1,0:T(8,128)(2,1)}, bf16[256,2048]{1,0:T(8,128)(2,1)}, bf16[2048,256]{1,0:T(8,128)(2,1)}) custom-call(bf16[128,2048]{1,0:T(8,128)(2,1)} %x_ref.1, bf16[128,2048]{1,0:T(8,128)(2,1)} %c_ref.1, bf16[256,2048]{1,0:T(8,128)(2,1)} %u_ref.1, bf16[2048,256]{1,0:T(8,128)(2,1)} %d_ref.1), custom_call_target="tpu_custom_call" | custom-call | tf_op jit(solution)/shard_map/pallas_call | solution.py:1089
  118.8 3.3 %shard_map.68 = (bf16[128,2048]{1,0:T(8,128)(2,1)}, f32[256,2048]{1,0:T(8,128)}, f32[2048,256]{1,0:T(8,128)}) custom-call(bf16[128,2048]{1,0:T(8,128)(2,1)} %get-tuple-element.6.refs_0_, bf16[256,2048]{1,0:T(8,128)(2,1)} %get-tuple-element.7.refs_1_, bf16[2048,256]{1,0:T(8,128)(2,1)} %get-tuple-element.8.refs_2_), custom_call_target="tpu_custom_call" | custom-call | tf_op jit(solution)/shard_map/pallas_call | solution.py:1026
